TPU v7x, 128 devices: a whole 4x4x4 slice. The times are simulated.
128 devices in a mesh: ep: 128 (over z, y, x, core).
Axes of the slice: x: 4, y: 4, z: 4, core: 2. Of those that a mesh axis runs over, the one named last changes fastest.
Arguments:
- tokens: bfloat16 [1024, 2048], P('ep'), may hold values from -6 to 6
- cache_keys: bfloat16 [1024, 1024, 128], P('ep'), may hold values from -80 to 80
- cache_values: bfloat16 [1024, 1024, 128], P('ep'), may hold values from -6 to 6
- cum_gates: float32 [1024, 1024, 2], P('ep'), may hold values from -1024 to 0, as said below
- lengths: int32 [1024], P('ep'), may hold values from 128 to 1024
- query_weight: bfloat16 [2048, 2048], replicated, may hold values from -0.125 to 0.125
- key_weight: bfloat16 [2048, 128], replicated, may hold values from -0.125 to 0.125
- value_weight: bfloat16 [2048, 128], replicated, may hold values from -0.125 to 0.125
- forget_weight: bfloat16 [2048, 2], replicated, may hold values from -0.125 to 0.125
- out_weight: bfloat16 [2048, 2048], P('ep'), may hold values from -1 to 1
- norm_gain: float32 [2, 2048], replicated, may hold values from 0.1 to 1.9
- norm_bias: float32 [2, 2048], replicated, may hold values from -1 to 1
- dense_gate_weight: bfloat16 [2048, 5632], P(None, 'ep'), may hold values from -0.125 to 0.125
- dense_up_weight: bfloat16 [2048, 5632], P(None, 'ep'), may hold values from -0.125 to 0.125
- dense_down_weight: bfloat16 [5632, 2048], P('ep'), may hold values from -0.078125 to 0.078125
- dense_scale: float32 [2048], replicated, may hold values from 0.2 to 1.5
- expert_gate_weight: bfloat16 [2048, 57344], P(None, 'ep'), may hold values from -0.125 to 0.125
- expert_up_weight: bfloat16 [2048, 57344], P(None, 'ep'), may hold values from -0.125 to 0.125
- expert_down_weight: bfloat16 [57344, 2048], P('ep'), may hold values from -0.0625 to 0.0625
- routes: int32 [1024, 2], replicated, may hold values from 0 to 7, all different within a row; in each aligned block of 8 rows (0 to 7, 8 to 15, ...) at most 3 rows name the same one
- route_weights: float32 [1024, 2], replicated, may hold values from 0.2 to 1
Outputs:
- output: bfloat16 [1024, 2048], P('ep')
Inputs may be any that keep to these rules, and one draw needn't show every extreme that they name: `routes`: each row names 2 different experts; the rows of one device (8 aligned rows) name one expert at most 3 times. `cum_gates`: non-increasing along positions.
All inputs are finite; a program needn't handle non-finite values.
Results may differ from a plain program's by a relative error of at most 0.012.
Values may be sent and summed in bfloat16 or wider, within the bound.
A program may use at most 128 MiB of HBM per device.

v0:
```python
import jax
import jax.numpy as jnp
from jax import lax
from jax.sharding import PartitionSpec as P

EXPERTS = 8
TOP = 2
CAP = 3


residual_scale = 1.4142135
norm_eps = 1e-05


def partner_2(block, axis, stride):
    count = lax.axis_size(axis)
    route = []
    for low in range(count):
        high = low | 1 << stride
        if high != low and high < count:
            route += [(low, high), (high, low)]
    return lax.ppermute(block, axis, route)


def layer_norm(values, gain_row, shift_row):
    centre = jnp.mean(values, axis=-1, keepdims=True)
    centred = values - centre
    spread = jnp.mean(centred * centred, axis=-1, keepdims=True)
    return (centred * lax.rsqrt(spread + norm_eps) * gain_row + shift_row).astype(jnp.bfloat16)


def attend(
    queries, cached_keys, cached_values, gate_sums, length_row, fresh_key, fresh_value, fresh_gate
):
    amount = queries.shape[0]
    cache_len = cached_keys.shape[1]
    kv_count = fresh_gate.shape[1]
    head_dim = fresh_key.shape[1] // kv_count
    grouped = queries.shape[1] // (kv_count * head_dim)
    query_grid_four = queries.reshape(amount, kv_count, grouped, head_dim)
    key_four = cached_keys.reshape(amount, cache_len, kv_count, head_dim)
    value_four = cached_values.reshape(amount, cache_len, kv_count, head_dim)
    self_key_row = fresh_key.reshape(amount, kv_count, head_dim)
    own_value = fresh_value.astype(jnp.float32).reshape(amount, kv_count, head_dim)
    ratio_value = head_dim ** (-0.5)
    latest = jnp.take_along_axis(gate_sums, (length_row - 1)[:, None, None], axis=1)
    offsets = jnp.transpose(latest - gate_sums + fresh_gate[:, None, :], (0, 2, 1))
    past = jnp.einsum(
        "bkgd,blkd->bkgl", query_grid_four, key_four, preferred_element_type=jnp.float32
    )
    past = past * ratio_value + offsets[:, :, None, :]
    live = jnp.arange(cache_len, dtype=jnp.int32)[None, :] < length_row[:, None]
    past = jnp.where(live[:, None, None, :], past, -jnp.inf)
    self_part = (
        jnp.einsum(
            "rifs,ris->rif", query_grid_four, self_key_row, preferred_element_type=jnp.float32
        )
        * ratio_value
    )
    highest = jnp.maximum(jnp.max(past, axis=-1), self_part)
    past_exp = jnp.exp(past - highest[..., None])
    own_exp = jnp.exp(self_part - highest)
    denominator = jnp.sum(past_exp, axis=-1) + own_exp
    past_weight = (past_exp / denominator[..., None]).astype(jnp.bfloat16)
    own_weight = (own_exp / denominator).astype(jnp.bfloat16)
    mixed = jnp.einsum(
        "bkgl,blkd->bkgd", past_weight, value_four, preferred_element_type=jnp.float32
    )
    mixed = mixed + own_weight.astype(jnp.float32)[..., None] * own_value[:, :, None, :]
    return mixed.reshape(amount, queries.shape[1]).astype(jnp.bfloat16)


def slot_tables(chosen, shares):
    expert_ids = jnp.arange(EXPERTS, dtype=jnp.int32)
    picked = (chosen[..., None] == expert_ids).astype(jnp.int32)
    hits = jnp.sum(picked, axis=2)
    portion = jnp.sum(picked.astype(jnp.float32) * shares[..., None], axis=2)
    ranks = jnp.cumsum(hits, axis=1) - hits
    slot_ids = jnp.arange(CAP, dtype=jnp.int32)
    matched = (hits[..., None] * (ranks[..., None] == slot_ids).astype(jnp.int32)).astype(
        jnp.float32
    )
    return (matched, portion)


def expert_part(inputs, gate_cols, up_cols, down_rows):
    gate_val = jnp.dot(inputs, gate_cols, preferred_element_type=jnp.float32)
    up_val = jnp.dot(inputs, up_cols, preferred_element_type=jnp.float32)
    hidden = (jax.nn.silu(gate_val) * up_val).astype(jnp.bfloat16)
    return jnp.dot(hidden, down_rows, preferred_element_type=jnp.float32).astype(jnp.bfloat16)


def experts_by_exchange(
    settled,
    routes,
    route_weights,
    own_index,
    shards,
    expert_gate_weight,
    expert_up_weight,
    expert_down_weight,
):
    rows_here = settled.shape[0]
    model_width = settled.shape[1]
    own_routes = lax.dynamic_slice_in_dim(routes, own_index * rows_here, rows_here, 0)
    own_shares = lax.dynamic_slice_in_dim(route_weights, own_index * rows_here, rows_here, 0)
    matched, portion = slot_tables(
        own_routes.reshape(1, rows_here, TOP), own_shares.reshape(1, rows_here, TOP)
    )
    matched = matched[0]
    portion = portion[0]
    send_slots = jnp.einsum(
        "sec,sd->ecd", matched.astype(jnp.bfloat16), settled, preferred_element_type=jnp.float32
    ).astype(jnp.bfloat16)
    outgoing = jnp.repeat(send_slots, shards, axis=0)
    received = lax.all_to_all(outgoing, "ep", split_axis=0, concat_axis=0, tiled=True)
    flat = received.reshape(-1, model_width)
    result = expert_part(flat, expert_gate_weight, expert_up_weight, expert_down_weight)
    answered = result.reshape(received.shape)
    returned = lax.all_to_all(answered, "ep", split_axis=0, concat_axis=0, tiled=True)
    summed = jnp.sum(
        returned.reshape(EXPERTS, shards, CAP, model_width).astype(jnp.float32), axis=1
    )
    return jnp.einsum("sec,ecd->sd", matched * portion[..., None], summed)


def local(
    tokens,
    cache_keys,
    cache_values,
    cum_gates,
    lengths,
    query_weight,
    key_weight,
    value_weight,
    forget_weight,
    out_weight,
    norm_gain,
    norm_bias,
    dense_gate_weight,
    dense_up_weight,
    dense_down_weight,
    dense_scale,
    expert_gate_weight,
    expert_up_weight,
    expert_down_weight,
    routes,
    route_weights,
):
    devices = lax.axis_size("ep")
    shards = devices // EXPERTS
    shard_bits = shards.bit_length() - 1
    total_bits = devices.bit_length() - 1
    own_index = lax.axis_index("ep")
    stacked = jnp.stack([dense_gate_weight, dense_up_weight, jnp.transpose(dense_down_weight)])
    for bit in range(shard_bits, total_bits):
        partner = partner_2(stacked, "ep", bit)
        upper = own_index >> bit & 1 == 1
        stacked = jnp.where(
            upper,
            jnp.concatenate([partner, stacked], axis=2),
            jnp.concatenate([stacked, partner], axis=2),
        )
    query = jnp.dot(tokens, query_weight, preferred_element_type=jnp.float32).astype(jnp.bfloat16)
    new_key = jnp.dot(tokens, key_weight, preferred_element_type=jnp.float32).astype(jnp.bfloat16)
    new_value = jnp.dot(tokens, value_weight, preferred_element_type=jnp.float32).astype(
        jnp.bfloat16
    )
    new_gate = jax.nn.log_sigmoid(
        jnp.dot(tokens, forget_weight, preferred_element_type=jnp.float32)
    )
    attended = attend(
        query, cache_keys, cache_values, cum_gates, lengths, new_key, new_value, new_gate
    )
    projected = jnp.dot(
        attended,
        lax.all_gather(out_weight, "ep", axis=0, tiled=True),
        preferred_element_type=jnp.float32,
    )
    settled = layer_norm(
        residual_scale * tokens.astype(jnp.float32) + projected, norm_gain[0], norm_bias[0]
    )
    group_rows = settled
    for bit in range(shard_bits):
        partner_rows = partner_2(group_rows, "ep", bit)
        upper = own_index >> bit & 1 == 1
        group_rows = jnp.where(
            upper,
            jnp.concatenate([partner_rows, group_rows], axis=0),
            jnp.concatenate([group_rows, partner_rows], axis=0),
        )
    dense_gate = jnp.dot(group_rows, stacked[0], preferred_element_type=jnp.float32)
    dense_up = jnp.dot(group_rows, stacked[1], preferred_element_type=jnp.float32)
    dense_hidden = (jax.nn.silu(dense_gate) * dense_up).astype(jnp.bfloat16)
    running = jnp.einsum("rf,df->rd", dense_hidden, stacked[2], preferred_element_type=jnp.float32)
    for bit in reversed(range(shard_bits)):
        half = running.shape[0] // 2
        upper = own_index >> bit & 1 == 1
        keep = jnp.where(upper, running[half:], running[:half])
        give = jnp.where(upper, running[:half], running[half:])
        running = keep + partner_2(give.astype(jnp.bfloat16), "ep", bit).astype(give.dtype)
    local_expert = experts_by_exchange(
        settled,
        routes,
        route_weights,
        own_index,
        shards,
        expert_gate_weight,
        expert_up_weight,
        expert_down_weight,
    )
    ffn = dense_scale * running + local_expert
    return layer_norm(
        residual_scale * settled.astype(jnp.float32) + ffn, norm_gain[1], norm_bias[1]
    )


def solution(mesh):
    return jax.shard_map(
        local,
        mesh=mesh,
        in_specs=(
            P("ep", None),
            P("ep", None, None),
            P("ep", None, None),
            P("ep", None, None),
            P("ep"),
            P(),
            P(),
            P(),
            P(),
            P("ep", None),
            P(),
            P(),
            P(None, "ep"),
            P(None, "ep"),
            P("ep", None),
            P(),
            P(None, "ep"),
            P(None, "ep"),
            P("ep", None),
            P(),
            P(),
        ),
        out_specs=P("ep", None),
        check_vma=False,
    )
```

profile of v0, /device:TPU:0, one launch (start us, length us, event | category | flops | bytes accessed | tf_op | source)
XLA Modules:
  0.0 263.8 jit_solution(18136717045035868061)
XLA Ops:
  8.5 3.4 %collective-permute-start.4 = (bf16[3,2048,44]{1,2,0:T(8,128)(2,1)S(1)}, bf16[3,2048,44]{1,2,0:T(8,128)(2,1)S(1)}, u32[]{:S(2)}, u32[]{:S(2)}) collective-permute-start(bf16[3,2048,44]{1,2,0:T(8,128)(2,1)S(1)} %pad_maximum_fusion), channel_id=1, source_target_pairs={{0,16},{16,0},{1,17},{17,1},{2,18},{18,2},{3,19},{19,3},{4,20},{20... | collective-permute-start | bytes 1622024 | tf_op jit(solution)/shard_map/ppermute | solution.py:22
  11.9 3.9 %copy.50 = bf16[8,1024,128]{1,2,0:T(8,128)(2,1)} copy(bf16[8,1024,128]{2,1,0:T(8,128)(2,1)} %param.23) | data formatting | bytes 4194304 | tf_op args[2]
  16.0 2.6 copy.48
  18.6 4.6 %convolution_convert_fusion.2 = bf16[8,2048]{1,0:T(8,128)(2,1)S(1)} fusion(bf16[8,2048]{1,0:T(8,128)(2,1)S(1)} %copy-done.5, bf16[2048,2048]{1,0:T(8,128)(2,1)} %param.26), kind=kOutput, calls=%fused_computation.7 | convolution fusion | flops 67125248 | bytes 8454144 | tf_op jit(solution)/shard_map/dot_general | solution.py:164
  23.4 3.9 %copy.47 = bf16[8,1024,128]{1,2,0:T(8,128)(2,1)} copy(bf16[8,1024,128]{2,1,0:T(8,128)(2,1)} %param.22) | data formatting | bytes 4194304 | tf_op args[1]
  30.0 1.3 gather_fusion
  31.7 2.1 fusion.46
  34.6 2.0 collective-permute-start.5
  37.6 25.5 %collective-permute-done.5 = bf16[3,2048,88]{1,2,0:T(8,128)(2,1)} collective-permute-done((bf16[3,2048,88]{1,2,0:T(8,128)(2,1)S(1)}, bf16[3,2048,88]{1,2,0:T(8,128)(2,1)}, u32[]{:S(2)}, u32[]{:S(2)}) %collective-permute-start.5) | collective-permute-done | bytes 1081376 | tf_op jit(solution)/shard_map/ppermute | solution.py:22
  63.1 4.5 %maximum_select_fusion.1 = bf16[3,2048,176]{1,2,0:T(8,128)(2,1)} fusion(bf16[3,2048,88]{1,2,0:T(8,128)(2,1)S(1)} %maximum_select_fusion.2, bf16[3,2048,88]{1,2,0:T(8,128)(2,1)} %collective-permute-done.5, pred[]{:T(512)S(6)} %eq.71), kind=kLoop, calls=%fused_computation.8 | loop fusion | flops 9732096 | bytes 4325377 | tf_op jit(solution)/shard_map/jit(_where)/select_n | solution.py:159
  67.5 3.5 %collective-permute-start.6 = (bf16[3,2048,176]{1,2,0:T(8,128)(2,1)}, bf16[3,2048,176]{1,2,0:T(8,128)(2,1)}, u32[]{:S(2)}, u32[]{:S(2)}) collective-permute-start(bf16[3,2048,176]{1,2,0:T(8,128)(2,1)} %maximum_select_fusion.1), channel_id=1, source_target_pairs={{0,64},{64,0},{1,65},{65,1},{2,66},{66,2},{3,67},{67,3},{4,68},{68... | collective-permute-start | bytes 6488072 | tf_op jit(solution)/shard_map/ppermute | solution.py:22
  71.0 52.6 %all-gather.2.cloned.1.call-done = bf16[2048,2048]{1,0:T(8,128)(2,1)} async-done(((bf16[16,2048]{1,0:T(8,128)(2,1)}), bf16[2048,2048]{1,0:T(8,128)(2,1)}) %all-gather.2.cloned.1.call-update) | async-done | bytes 8388624 | tf_op jit(solution)/shard_map/all_gather | solution.py:177
  123.6 4.7 %fusion.47 = (f32[8]{0:T(128)S(1)}, f32[8,2048]{1,0:T(8,128)S(1)}) fusion(bf16[8,2048]{1,0:T(8,128)(2,1)S(1)} %convert_element_type.123, bf16[2048,2048]{1,0:T(8,128)(2,1)} %all-gather.2.cloned.1.call-done, bf16[8,2048]{1,0:T(8,128)(2,1)S(1)} %copy-done.5), kind=kOutput, calls=%fused_computation.107 | convolution fusion | flops 67174392 | bytes 8519712 | tf_op jit(solution)/shard_map/dot_general | solution.py:175
  129.9 1.5 collective-permute-start.1
  131.5 2.8 %collective-permute-done.1 = bf16[16,2048]{1,0:T(8,128)(2,1)S(1)} collective-permute-done((bf16[16,2048]{1,0:T(8,128)(2,1)S(1)}, bf16[16,2048]{1,0:T(8,128)(2,1)S(1)}, u32[]{:S(2)}, u32[]{:S(2)}) %collective-permute-start.1) | collective-permute-done | bytes 65568 | tf_op jit(solution)/shard_map/ppermute | solution.py:22
  134.3 3.1 %collective-permute-start.2 = (bf16[32,2048]{1,0:T(8,128)(2,1)S(1)}, bf16[32,2048]{1,0:T(8,128)(2,1)S(1)}, u32[]{:S(2)}, u32[]{:S(2)}) collective-permute-start(bf16[32,2048]{1,0:T(8,128)(2,1)S(1)} %maximum_select_fusion.5), channel_id=1, source_target_pairs={{0,4},{4,0},{1,5},{5,1},{2,6},{6,2},{3,7},{7,3},{8,12},{12,8},{9,1... | collective-permute-start | bytes 393224 | tf_op jit(solution)/shard_map/ppermute | solution.py:22
  138.2 2.6 collective-permute-done.2
  141.9 6.2 %maximum_select_fusion = bf16[3,2048,352]{1,2,0:T(8,128)(2,1)} fusion(bf16[3,2048,176]{1,2,0:T(8,128)(2,1)} %maximum_select_fusion.1, bf16[3,2048,176]{1,2,0:T(8,128)(2,1)} %collective-permute-done.6, pred[]{:T(512)S(6)} %eq.70), kind=kLoop, calls=%fused_computation.1 | loop fusion | flops 19464192 | bytes 8650753 | tf_op jit(solution)/shard_map/jit(_where)/select_n | solution.py:159
  148.4 2.4 broadcast_in_dim.21
  150.8 12.5 %all-to-all-start = ((bf16[128,3,2048]{2,1,0:T(4,128)(2,1)}), bf16[128,3,2048]{2,1,0:T(4,128)(2,1)}, u32[]{:S(2)}, u32[]{:S(2)}) async-start(bf16[128,3,2048]{2,1,0:T(4,128)(2,1)} %bitcast.66), calls=%async_computation | async-start | bytes 4194304 | tf_op jit(solution)/shard_map/all_to_all | solution.py:116
  164.0 2.6 fusion.1
  166.6 3.5 %fusion = f32[128,2048]{1,0:T(8,128)S(1)} fusion(bf16[3,2048,352]{1,2,0:T(8,128)(2,1)} %maximum_select_fusion, f32[128,352]{0,1:T(8,128)} %fusion.1, bf16[64,2048]{1,0:T(8,128)(2,1)S(1)} %maximum_select_fusion.4, bf16[64,2048]{1,0:T(8,128)(2,1)} %copy-done.11, pred[]{:T(512)S(6)} %eq.69), kind=kOutput, calls=%fused_computation.10 | convolution fusion | flops 371728384 | bytes 4636673 | tf_op jit(solution)/shard_map/rf,df->rd/dot_general | solution.py:195
  171.7 20.2 %collective-permute-done.7 = bf16[64,2048]{1,0:T(8,128)(2,1)S(1)} collective-permute-done((bf16[64,2048]{1,0:T(8,128)(2,1)S(1)}, bf16[64,2048]{1,0:T(8,128)(2,1)S(1)}, u32[]{:S(2)}, u32[]{:S(2)}) %collective-permute-start.7) | collective-permute-done | bytes 262176 | tf_op jit(solution)/shard_map/ppermute | solution.py:22
  192.0 3.0 %collective-permute-start.8 = (bf16[32,2048]{1,0:T(8,128)(2,1)S(1)}, bf16[32,2048]{1,0:T(8,128)(2,1)S(1)}, u32[]{:S(2)}, u32[]{:S(2)}) collective-permute-start(bf16[32,2048]{1,0:T(8,128)(2,1)S(1)} %select_convert_fusion.1), channel_id=1, source_target_pairs={{0,4},{4,0},{1,5},{5,1},{2,6},{6,2},{3,7},{7,3},{8,12},{12,8},{9,1... | collective-permute-start | bytes 393224 | tf_op jit(solution)/shard_map/ppermute | solution.py:22
  195.1 5.0 %reshape.158 = bf16[384,2048]{1,0:T(8,128)(2,1)} reshape(bf16[128,3,2048]{2,1,0:T(4,128)(2,1)} %all-to-all-done) | data formatting | bytes 3145728 | tf_op jit(solution)/shard_map/reshape | solution.py:117
  200.1 3.1 %fusion.49 = f32[384,448]{0,1:T(8,128)S(1)} fusion(bf16[384,2048]{1,0:T(8,128)(2,1)} %reshape.158, bf16[2048,448]{0,1:T(8,128)(2,1)} %param.37), kind=kOutput, calls=%fused_computation.109 | convolution fusion | flops 704643072 | bytes 4096000 | tf_op jit(solution)/shard_map/dot_general | solution.py:87
  203.2 5.2 %convolution_convert_fusion = bf16[384,2048]{1,0:T(8,128)(2,1)} fusion(bf16[448,2048]{1,0:T(8,128)(2,1)S(1)} %copy-done, bf16[384,2048]{1,0:T(8,128)(2,1)} %reshape.158, bf16[2048,448]{0,1:T(8,128)(2,1)} %param.38, f32[384,448]{0,1:T(8,128)S(1)} %fusion.49), kind=kOutput, calls=%fused_computation.3 | convolution fusion | flops 1411104768 | bytes 7503872 | tf_op jit(solution)/shard_map/dot_general | solution.py:90
  208.5 5.1 %reshape.159 = bf16[128,3,2048]{2,1,0:T(4,128)(2,1)} reshape(bf16[384,2048]{1,0:T(8,128)(2,1)} %convolution_convert_fusion) | data formatting | bytes 3145728 | tf_op jit(solution)/shard_map/reshape | solution.py:119
  213.6 8.7 %all-to-all-start.1 = ((bf16[128,3,2048]{2,1,0:T(4,128)(2,1)}), bf16[128,3,2048]{2,1,0:T(4,128)(2,1)}, u32[]{:S(2)}, u32[]{:S(2)}) async-start(bf16[128,3,2048]{2,1,0:T(4,128)(2,1)} %reshape.159), calls=%async_computation.1 | async-start | bytes 4194304 | tf_op jit(solution)/shard_map/all_to_all | solution.py:120
  223.5 23.5 %collective-permute-done.9 = bf16[16,2048]{1,0:T(8,128)(2,1)S(1)} collective-permute-done((bf16[16,2048]{1,0:T(8,128)(2,1)S(1)}, bf16[16,2048]{1,0:T(8,128)(2,1)S(1)}, u32[]{:S(2)}, u32[]{:S(2)}) %collective-permute-start.9) | collective-permute-done | bytes 65568 | tf_op jit(solution)/shard_map/ppermute | solution.py:22
  247.1 5.8 %all-to-all-done.1 = bf16[128,3,2048]{2,1,0:T(4,128)(2,1)} async-done(((bf16[128,3,2048]{2,1,0:T(4,128)(2,1)}), bf16[128,3,2048]{2,1,0:T(4,128)(2,1)}, u32[]{:S(2)}, u32[]{:S(2)}) %all-to-all-start.1) | async-done | bytes 1572896 | tf_op jit(solution)/shard_map/all_to_all | solution.py:120
  252.9 2.7 %convert_reduce_fusion = bf16[8,3,2048]{2,1,0:T(4,128)(2,1)S(1)} fusion(bf16[128,3,2048]{2,1,0:T(4,128)(2,1)} %all-to-all-done.1), kind=kLoop, calls=%fused_computation.2 | loop fusion | flops 1523712 | bytes 1671168 | tf_op jit(solution)/shard_map/reduce_sum | solution.py:121
  (93 shorter events, 15.8 us)
Async XLA Ops:
  6.5 196.7 %copy-start = (bf16[448,2048]{1,0:T(8,128)(2,1)S(1)}, bf16[448,2048]{1,0:T(8,128)(2,1)}, u32[]{:S(2)}) copy-start(bf16[448,2048]{1,0:T(8,128)(2,1)} %param.39) | copy-start | bytes 5505028
  6.5 117.1 %all-gather.2.cloned.1.call-start = ((), (), s32[]{:S(2)}) async-start(), calls=%async_computation.2 | async-start | bytes 8454144 | tf_op jit(solution)/shard_map/all_gather | solution.py:177
  8.5 7.3 %copy-start.5 = (bf16[8,2048]{1,0:T(8,128)(2,1)S(1)}, bf16[8,2048]{1,0:T(8,128)(2,1)}, u32[]{:S(2)}) copy-start(bf16[8,2048]{1,0:T(8,128)(2,1)} %param.21) | copy-start | bytes 98308
  8.5 7.3 %copy-start.12 = (bf16[2048,2]{0,1:T(2,128)(2,1)S(1)}, bf16[2048,2]{0,1:T(2,128)(2,1)}, u32[]{:S(2)}) copy-start(bf16[2048,2]{0,1:T(2,128)(2,1)} %param.29) | copy-start | bytes 24580
  8.5 7.5 %copy-start.6 = (f32[8,1024,2]{1,2,0:T(2,128)S(1)}, f32[8,1024,2]{1,2,0:T(2,128)}, u32[]{:S(2)}) copy-start(f32[8,1024,2]{1,2,0:T(2,128)} %param.24) | copy-start | bytes 196612
  8.5 25.7 %collective-permute-start.4 = (bf16[3,2048,44]{1,2,0:T(8,128)(2,1)S(1)}, bf16[3,2048,44]{1,2,0:T(8,128)(2,1)S(1)}, u32[]{:S(2)}, u32[]{:S(2)}) collective-permute-start(bf16[3,2048,44]{1,2,0:T(8,128)(2,1)S(1)} %pad_maximum_fusion), channel_id=1, source_target_pairs={{0,16},{16,0},{1,17},{17,1},{2,18},{18,2},{3,19},{19,3},{4,20},{20... | collective-permute-start | bytes 1622024 | tf_op jit(solution)/shard_map/ppermute | solution.py:22
  23.3 6.6 %copy-start.10 = (s32[8]{0:T(128)S(1)}, s32[8]{0:T(128)}, u32[]{:S(2)}) copy-start(s32[8]{0:T(128)} %param.25) | copy-start | bytes 100
  31.6 2.6 copy-start.2
  31.6 2.6 copy-start.3
  31.7 2.6 copy-start.4
  33.8 2.8 %copy-start.1 = (bf16[8,1024,128]{1,2,0:T(8,128)(2,1)S(1)}, bf16[8,1024,128]{1,2,0:T(8,128)(2,1)}, u32[]{:S(2)}) copy-start(bf16[8,1024,128]{1,2,0:T(8,128)(2,1)} %copy.50) | copy-start | bytes 6291460
  34.6 28.4 %collective-permute-start.5 = (bf16[3,2048,88]{1,2,0:T(8,128)(2,1)S(1)}, bf16[3,2048,88]{1,2,0:T(8,128)(2,1)}, u32[]{:S(2)}, u32[]{:S(2)}) collective-permute-start(bf16[3,2048,88]{1,2,0:T(8,128)(2,1)S(1)} %maximum_select_fusion.2), channel_id=1, source_target_pairs={{0,32},{32,0},{1,33},{33,1},{2,34},{34,2},{3,35},{35,3},{4,36},{36... | collective-permute-start | bytes 3244040 | tf_op jit(solution)/shard_map/ppermute | solution.py:22
  36.6 0.9 copy-start.7
  36.6 0.9 copy-start.8
  67.5 74.4 %collective-permute-start.6 = (bf16[3,2048,176]{1,2,0:T(8,128)(2,1)}, bf16[3,2048,176]{1,2,0:T(8,128)(2,1)}, u32[]{:S(2)}, u32[]{:S(2)}) collective-permute-start(bf16[3,2048,176]{1,2,0:T(8,128)(2,1)} %maximum_select_fusion.1), channel_id=1, source_target_pairs={{0,64},{64,0},{1,65},{65,1},{2,66},{66,2},{3,67},{67,3},{4,68},{68... | collective-permute-start | bytes 6488072 | tf_op jit(solution)/shard_map/ppermute | solution.py:22
  128.6 1.3 collective-permute-start
  129.9 4.3 %collective-permute-start.1 = (bf16[16,2048]{1,0:T(8,128)(2,1)S(1)}, bf16[16,2048]{1,0:T(8,128)(2,1)S(1)}, u32[]{:S(2)}, u32[]{:S(2)}) collective-permute-start(bf16[16,2048]{1,0:T(8,128)(2,1)S(1)} %maximum_select_fusion.9), channel_id=1, source_target_pairs={{0,2},{2,0},{1,3},{3,1},{4,6},{6,4},{5,7},{7,5},{8,10},{10,8},{9,1... | collective-permute-start | bytes 196616 | tf_op jit(solution)/shard_map/ppermute | solution.py:22
  134.3 6.6 %collective-permute-start.2 = (bf16[32,2048]{1,0:T(8,128)(2,1)S(1)}, bf16[32,2048]{1,0:T(8,128)(2,1)S(1)}, u32[]{:S(2)}, u32[]{:S(2)}) collective-permute-start(bf16[32,2048]{1,0:T(8,128)(2,1)S(1)} %maximum_select_fusion.5), channel_id=1, source_target_pairs={{0,4},{4,0},{1,5},{5,1},{2,6},{6,2},{3,7},{7,3},{8,12},{12,8},{9,1... | collective-permute-start | bytes 393224 | tf_op jit(solution)/shard_map/ppermute | solution.py:22
  140.9 22.4 %collective-permute-start.3 = (bf16[64,2048]{1,0:T(8,128)(2,1)S(1)}, bf16[64,2048]{1,0:T(8,128)(2,1)S(1)}, u32[]{:S(2)}, u32[]{:S(2)}) collective-permute-start(bf16[64,2048]{1,0:T(8,128)(2,1)S(1)} %maximum_select_fusion.4), channel_id=1, source_target_pairs={{0,8},{8,0},{1,9},{9,1},{2,10},{10,2},{3,11},{11,3},{4,12},{12,4},... | collective-permute-start | bytes 786440 | tf_op jit(solution)/shard_map/ppermute | solution.py:22
  150.8 44.3 %all-to-all-start = ((bf16[128,3,2048]{2,1,0:T(4,128)(2,1)}), bf16[128,3,2048]{2,1,0:T(4,128)(2,1)}, u32[]{:S(2)}, u32[]{:S(2)}) async-start(bf16[128,3,2048]{2,1,0:T(4,128)(2,1)} %bitcast.66), calls=%async_computation | async-start | bytes 4194304 | tf_op jit(solution)/shard_map/all_to_all | solution.py:116
  163.3 0.7 copy-start.11
  170.2 21.8 %collective-permute-start.7 = (bf16[64,2048]{1,0:T(8,128)(2,1)S(1)}, bf16[64,2048]{1,0:T(8,128)(2,1)S(1)}, u32[]{:S(2)}, u32[]{:S(2)}) collective-permute-start(bf16[64,2048]{1,0:T(8,128)(2,1)S(1)} %select_convert_fusion), channel_id=1, source_target_pairs={{0,8},{8,0},{1,9},{9,1},{2,10},{10,2},{3,11},{11,3},{4,12},{12,4},... | collective-permute-start | bytes 786440 | tf_op jit(solution)/shard_map/ppermute | solution.py:22
  192.0 30.3 %collective-permute-start.8 = (bf16[32,2048]{1,0:T(8,128)(2,1)S(1)}, bf16[32,2048]{1,0:T(8,128)(2,1)S(1)}, u32[]{:S(2)}, u32[]{:S(2)}) collective-permute-start(bf16[32,2048]{1,0:T(8,128)(2,1)S(1)} %select_convert_fusion.1), channel_id=1, source_target_pairs={{0,4},{4,0},{1,5},{5,1},{2,6},{6,2},{3,7},{7,3},{8,12},{12,8},{9,1... | collective-permute-start | bytes 393224 | tf_op jit(solution)/shard_map/ppermute | solution.py:22
  213.6 39.2 %all-to-all-start.1 = ((bf16[128,3,2048]{2,1,0:T(4,128)(2,1)}), bf16[128,3,2048]{2,1,0:T(4,128)(2,1)}, u32[]{:S(2)}, u32[]{:S(2)}) async-start(bf16[128,3,2048]{2,1,0:T(4,128)(2,1)} %reshape.159), calls=%async_computation.1 | async-start | bytes 4194304 | tf_op jit(solution)/shard_map/all_to_all | solution.py:120
  222.4 33.4 %copy-start.9 = (f32[2048]{0:T(1024)S(1)}, f32[2048]{0:T(1024)}, u32[]{:S(2)}) copy-start(f32[2048]{0:T(1024)} %param.36) | copy-start | bytes 24580
  222.5 24.5 %collective-permute-start.9 = (bf16[16,2048]{1,0:T(8,128)(2,1)S(1)}, bf16[16,2048]{1,0:T(8,128)(2,1)S(1)}, u32[]{:S(2)}, u32[]{:S(2)}) collective-permute-start(bf16[16,2048]{1,0:T(8,128)(2,1)S(1)} %select_convert_fusion.2), channel_id=1, source_target_pairs={{0,2},{2,0},{1,3},{3,1},{4,6},{6,4},{5,7},{7,5},{8,10},{10,8},{9,1... | collective-permute-start | bytes 196616 | tf_op jit(solution)/shard_map/ppermute | solution.py:22
  247.0 8.8 %collective-permute-start.10 = (bf16[8,2048]{1,0:T(8,128)(2,1)S(1)}, bf16[8,2048]{1,0:T(8,128)(2,1)S(1)}, u32[]{:S(2)}, u32[]{:S(2)}) collective-permute-start(bf16[8,2048]{1,0:T(8,128)(2,1)S(1)} %select_convert_fusion.3), channel_id=1, source_target_pairs={{0,1},{1,0},{2,3},{3,2},{4,5},{5,4},{6,7},{7,6},{8,9},{9,8},{10,11... | collective-permute-start | bytes 98312 | tf_op jit(solution)/shard_map/ppermute | solution.py:22
Sparse Core Ops, SparseCore 0:
  10.3 113.2 all-gather.1
where the time goes:
time: 265 us; the launch traced here: 264 us
  waiting for transfers between devices  135 us (51%)
  starting transfers between devices  40.8 us (15%)
  matrix products  29.7 us (11%)
  local copies, waits for them, and re-layouts  27.2 us (10%)
  other arithmetic  17.5 us (7%)
  between operations  13.8 us (5%)
    ppermute x11, waiting for transfers between devices, partner_2(): return lax.ppermute(block, axis, route)  75.8 us
    all_gather x1, waiting for transfers between devices, local(): lax.all_gather(out_weight, 'ep', axis=0, tiled=True)  52.6 us
    ppermute x11, starting transfers between devices, partner_2(): return lax.ppermute(block, axis, route)  19.6 us
    all_to_all x1, starting transfers between devices, experts_by_exchange(): lax.all_to_all(outgoing, 'ep', split_axis=0, concat_axis=0, tiled=True)  12.5 us
    unnamed x30, local copies, waits for them, and re-layouts  11.2 us
    select_n x3, other arithmetic, local(): jnp.where(upper, jnp.concatenate([partner, stacked], axis=2), jnp.concate...  11 us
    all_to_all x1, starting transfers between devices, experts_by_exchange(): lax.all_to_all(answered, 'ep', split_axis=0, concat_axis=0, tiled=True)  8.74 us
    all_to_all x1, waiting for transfers between devices, experts_by_exchange(): lax.all_to_all(answered, 'ep', split_axis=0, concat_axis=0, tiled=True)  5.76 us
  transfers between devices with their start and end apart: 14, of which 8 were waited for; matrix products, arithmetic and copies ran while one was open for 27% of the time, Pallas kernels for 0%

commit v1 on v0

v1 whole, which is shorter than its diff:
```python
import functools

import jax
import jax.numpy as jnp
from jax import lax
from jax.experimental import pallas as pl
from jax.experimental.pallas import tpu as pltpu
from jax.sharding import PartitionSpec as P

MESH = pl.DeviceIdType.MESH
F32 = jnp.float32
BF16 = jnp.bfloat16
SIDE = 4
ROWS = 8
WIDTH = 2048
EXPERTS = 8
FFE = 448
FFD = 44
FFP = 512
CHUNKS = ((0, 768), (768, 640), (1408, 640))
GATHER_ORDER = ((2, 1, 0), (0, 2, 1), (1, 0, 2))
residual_scale = 1.4142135
norm_eps = 1e-05


def norm_rows(values, gain_row, shift_row):
    centre = jnp.mean(values, axis=-1, keepdims=True)
    centred = values - centre
    spread = jnp.mean(centred * centred, axis=-1, keepdims=True)
    return (centred * lax.rsqrt(spread + norm_eps) * gain_row + shift_row).astype(BF16)


def position():
    me = lax.axis_index("ep")
    core = me % 2
    x = (me // 2) % SIDE
    y = (me // (2 * SIDE)) % SIDE
    z = me // (2 * SIDE * SIDE)
    return core, (z, y, x)


def device_at(core, spot):
    z, y, x = spot
    return (((z * SIDE + y) * SIDE + x) * 2 + core,)


def moved(spot, dim, value):
    return tuple(value if d == dim else spot[d] for d in range(3))


def shifted(spot, dim, offset):
    return moved(spot, dim, (spot[dim] + offset + SIDE) % SIDE)


def columns(k):
    return pl.ds(CHUNKS[k][0], CHUNKS[k][1])


def remote(src, dst, send, recv, target):
    return pltpu.make_async_remote_copy(
        src_ref=src, dst_ref=dst, send_sem=send, recv_sem=recv, device_id=target, device_id_type=MESH
    )


def entry_barrier(core, spot):
    barrier = pltpu.get_barrier_semaphore()
    pl.semaphore_signal(barrier, inc=1, device_id=device_at(1 - core, spot), device_id_type=MESH)
    for dim in range(3):
        for offset in range(1, SIDE):
            pl.semaphore_signal(
                barrier, inc=1, device_id=device_at(core, shifted(spot, dim, offset)), device_id_type=MESH
            )
    pl.semaphore_wait(barrier, 3 * (SIDE - 1) + 1)


def gather_region(rows_ref, k, core, spot, done):
    where = tuple(pl.ds(0, SIDE) if d in done else spot[d] for d in range(3))
    return rows_ref.at[(core,) + where + (pl.ds(0, ROWS), columns(k))]


def gather_rows(rows_ref, core, spot, gsend, grecv, fsend, frecv, osend, orecv):
    started = []
    partner = device_at(1 - core, spot)
    own = rows_ref.at[(core,) + spot]
    copy = remote(own, own, osend, orecv, partner)
    copy.start()
    started.append(copy)

    def start(k, phase):
        order = GATHER_ORDER[k]
        region = gather_region(rows_ref, k, core, spot, order[:phase])
        for offset in range(1, SIDE):
            target = device_at(core, shifted(spot, order[phase], offset))
            copy = remote(
                region, region, gsend.at[k, phase, offset - 1], grecv.at[k, phase, offset - 1], target
            )
            copy.start()
            started.append(copy)

    def arrive(k, phase):
        order = GATHER_ORDER[k]
        for offset in range(1, SIDE):
            source = shifted(spot, order[phase], -offset)
            region = gather_region(rows_ref, k, core, source, order[:phase])
            remote(
                region, region, gsend.at[k, phase, offset - 1], grecv.at[k, phase, offset - 1],
                device_at(core, source),
            ).wait_recv()

    def forward(k, phase):
        order = GATHER_ORDER[k]
        for offset in range(1, SIDE):
            source = shifted(spot, order[phase], -offset)
            region = gather_region(rows_ref, k, core, source, order[:phase])
            copy = remote(
                region, region, fsend.at[k, phase, offset - 1], frecv.at[k, phase, offset - 1], partner
            )
            copy.start()
            started.append(copy)

    def forwarded(k, phase):
        order = GATHER_ORDER[k]
        for offset in range(1, SIDE):
            source = shifted(spot, order[phase], -offset)
            region = gather_region(rows_ref, k, 1 - core, source, order[:phase])
            remote(
                region, region, fsend.at[k, phase, offset - 1], frecv.at[k, phase, offset - 1], partner
            ).wait_recv()

    for k in range(3):
        start(k, 0)
    for phase in range(3):
        for k in range(3):
            arrive(k, phase)
            if phase < 2:
                start(k, phase + 1)
            forward(k, phase)
    other = rows_ref.at[(1 - core,) + spot]
    remote(other, other, osend, orecv, partner).wait_recv()
    for phase in range(3):
        for k in range(3):
            forwarded(k, phase)
    return started


def left_over(k, phase):
    gone = GATHER_ORDER[k][::-1][:phase]
    return [d for d in range(3) if d not in gone]


def ffn_kernel(
    settled_ref, routes_ref, shares_ref, gate_hbm, up_hbm, down_hbm, dgate_ref, dup_ref, ddown_ref,
    scale_ref, gain_ref, bias_ref, out_ref,
    rows_ref, wg_ref, wu_ref, wd_ref, factor_ref, part_ref, twin_ref, r0_ref, r1_ref, r2_ref, s1_ref, s2_ref,
    wsem, gsend, grecv, fsend, frecv, osend, orecv, tsend, trecv, rsend, rrecv,
):
    core, spot = position()
    entry_barrier(core, spot)
    loads = [
        pltpu.make_async_copy(gate_hbm, wg_ref.at[pl.ds(0, FFE)], wsem.at[0]),
        pltpu.make_async_copy(up_hbm, wu_ref.at[pl.ds(0, FFE)], wsem.at[1]),
        pltpu.make_async_copy(down_hbm, wd_ref.at[pl.ds(0, FFE)], wsem.at[2]),
    ]
    for load in loads:
        load.start()
    rows_ref[(core,) + spot] = settled_ref[...]
    pad = jnp.zeros((FFP - FFE - FFD, WIDTH), BF16)
    for ref, dense in ((wg_ref, dgate_ref[...]), (wu_ref, dup_ref[...])):
        ref[FFE:, :] = jnp.concatenate([dense, pad], axis=0)
    ddown = (ddown_ref[...].astype(F32) * scale_ref[...]).astype(BF16)
    wd_ref[FFE:, :] = jnp.concatenate([ddown, pad], axis=0)
    expert = lax.axis_index("ep") // (2 * SIDE * SIDE * SIDE // EXPERTS)
    picked = jnp.where(routes_ref[...] == expert, shares_ref[...], 0.0)
    factor = jnp.sum(picked, axis=0, keepdims=True)
    turned = jnp.transpose(jnp.broadcast_to(factor, (8, factor.shape[1])))
    factor_ref[...] = turned.reshape(factor_ref.shape)

    started = gather_rows(rows_ref, core, spot, gsend, grecv, fsend, frecv, osend, orecv)
    for load in loads:
        load.wait()

    nt = (((1,), (1,)), ((), ()))
    block = 2 * SIDE * SIDE * ROWS
    lane = lax.broadcasted_iota(jnp.int32, (1, FFP), 1)

    def part_of(half, plane):
        x = rows_ref.at[half, pl.ds(plane, 2)].reshape(block, WIDTH)[...]
        gate = lax.dot_general(x, wg_ref[...], nt, preferred_element_type=F32)
        up = lax.dot_general(x, wu_ref[...], nt, preferred_element_type=F32)
        weight = factor_ref[pl.ds(plane * SIDE * SIDE, 2 * SIDE * SIDE), half].reshape(block, 8)[:, :1]
        weight = jnp.where(lane < FFE, weight, 1.0)
        hidden = (gate * jax.nn.sigmoid(gate) * up * weight).astype(BF16)
        return jnp.dot(hidden, wd_ref[...], preferred_element_type=F32)

    partner = device_at(1 - core, spot)

    def twin_copy(i):
        return remote(
            part_ref.at[1 - core, pl.ds(2 * i, 2)], twin_ref.at[pl.ds(2 * i, 2)], tsend.at[i], trecv.at[i], partner
        )

    def far(i, carry):
        part_ref.at[1 - core, pl.ds(2 * i, 2)].reshape(block, WIDTH)[...] = part_of(1 - core, 2 * i).astype(BF16)
        twin_copy(i).start()
        return carry

    lax.fori_loop(0, SIDE // 2, far, 0)

    def near(i, carry):
        value = part_of(core, 2 * i)
        twin_copy(i).wait_recv()
        value = value + twin_ref.at[pl.ds(2 * i, 2)].reshape(block, WIDTH)[...].astype(F32)
        part_ref.at[core, pl.ds(2 * i, 2)].reshape(block, WIDTH)[...] = value.astype(BF16)
        return carry

    lax.fori_loop(0, SIDE // 2, near, 0)

    sums = ((part_ref, r0_ref, s1_ref), (s1_ref, r1_ref, s2_ref), (s2_ref, r2_ref, None))

    def slab(ref, phase, k, value):
        dims = left_over(k, phase)
        dim = GATHER_ORDER[k][::-1][phase]
        where = tuple(value if d == dim else pl.ds(0, SIDE) for d in dims)
        if phase == 0:
            where = (core,) + where
        return ref.at[where + (pl.ds(0, ROWS), columns(k))]

    def landed(ref, phase, k, index):
        where = (index,) + tuple(pl.ds(0, SIDE) for _ in range(2 - phase))
        return ref.at[where + (pl.ds(0, ROWS), columns(k))]

    def reduce_copy(phase, k, offset):
        dim = GATHER_ORDER[k][::-1][phase]
        target = shifted(spot, dim, offset)
        return remote(
            slab(sums[phase][0], phase, k, target[dim]), landed(sums[phase][1], phase, k, offset - 1),
            rsend.at[k, phase, offset - 1], rrecv.at[k, phase, offset - 1], device_at(core, target),
        )

    def reduce_start(phase, k):
        for offset in range(1, SIDE):
            copy = reduce_copy(phase, k, offset)
            copy.start()
            started.append(copy)

    def reduce_sum(phase, k):
        dim = GATHER_ORDER[k][::-1][phase]
        total = slab(sums[phase][0], phase, k, spot[dim])[...].astype(F32)
        for offset in range(1, SIDE):
            reduce_copy(phase, k, offset).wait_recv()
            total = total + landed(sums[phase][1], phase, k, offset - 1)[...].astype(F32)
        return total

    for k in range(3):
        reduce_start(0, k)
    for phase in range(2):
        for k in range(3):
            where = tuple(pl.ds(0, SIDE) for _ in range(2 - phase)) + (pl.ds(0, ROWS), columns(k))
            sums[phase][2][where] = reduce_sum(phase, k).astype(BF16)
            reduce_start(phase + 1, k)
    ffn = jnp.concatenate([reduce_sum(2, k) for k in range(3)], axis=-1)
    out_ref[...] = norm_rows(
        residual_scale * settled_ref[...].astype(F32) + ffn, gain_ref[1:2, :], bias_ref[1:2, :]
    )
    for copy in started:
        copy.wait_send()
    for i in range(SIDE // 2):
        twin_copy(i).wait_send()


def ffn_call(settled, routes, shares, gate, up, down, dgate, dup, ddown, scale, gain, bias):
    vmem = pl.BlockSpec(memory_space=pltpu.VMEM)
    hbm = pl.BlockSpec(memory_space=pltpu.HBM)
    sem = pltpu.SemaphoreType.DMA
    cube = (SIDE, SIDE, SIDE, ROWS, WIDTH)
    return pl.pallas_call(
        ffn_kernel,
        out_shape=jax.ShapeDtypeStruct((ROWS, WIDTH), BF16),
        in_specs=[vmem, vmem, vmem, hbm, hbm, hbm, vmem, vmem, vmem, vmem, vmem, vmem],
        out_specs=vmem,
        scratch_shapes=[
            pltpu.VMEM((2,) + cube, BF16),
            pltpu.VMEM((FFP, WIDTH), BF16),
            pltpu.VMEM((FFP, WIDTH), BF16),
            pltpu.VMEM((FFP, WIDTH), BF16),
            pltpu.VMEM((SIDE**3, 2, ROWS, 8), F32),
            pltpu.VMEM((2,) + cube, BF16),
            pltpu.VMEM(cube, BF16),
            pltpu.VMEM((SIDE - 1,) + cube[1:], BF16),
            pltpu.VMEM((SIDE - 1,) + cube[2:], BF16),
            pltpu.VMEM((SIDE - 1,) + cube[3:], BF16),
            pltpu.VMEM(cube[1:], BF16),
            pltpu.VMEM(cube[2:], BF16),
            sem((3,)),
            sem((3, 3, SIDE - 1)), sem((3, 3, SIDE - 1)),
            sem((3, 3, SIDE - 1)), sem((3, 3, SIDE - 1)),
            sem, sem,
            sem((SIDE // 2,)), sem((SIDE // 2,)),
            sem((3, 3, SIDE - 1)), sem((3, 3, SIDE - 1)),
        ],
        compiler_params=pltpu.CompilerParams(
            collective_id=0, has_side_effects=True, vmem_limit_bytes=60 * 2**20
        ),
        name="ffn",
    )(settled, routes, shares, gate, up, down, dgate, dup, ddown, scale, gain, bias)


def layer_norm(values, gain_row, shift_row):
    return norm_rows(values, gain_row, shift_row)


def attend(
    queries, cached_keys, cached_values, gate_sums, length_row, fresh_key, fresh_value, fresh_gate
):
    amount = queries.shape[0]
    cache_len = cached_keys.shape[1]
    kv_count = fresh_gate.shape[1]
    head_dim = fresh_key.shape[1] // kv_count
    grouped = queries.shape[1] // (kv_count * head_dim)
    query_grid_four = queries.reshape(amount, kv_count, grouped, head_dim)
    key_four = cached_keys.reshape(amount, cache_len, kv_count, head_dim)
    value_four = cached_values.reshape(amount, cache_len, kv_count, head_dim)
    self_key_row = fresh_key.reshape(amount, kv_count, head_dim)
    own_value = fresh_value.astype(jnp.float32).reshape(amount, kv_count, head_dim)
    ratio_value = head_dim ** (-0.5)
    latest = jnp.take_along_axis(gate_sums, (length_row - 1)[:, None, None], axis=1)
    offsets = jnp.transpose(latest - gate_sums + fresh_gate[:, None, :], (0, 2, 1))
    past = jnp.einsum(
        "bkgd,blkd->bkgl", query_grid_four, key_four, preferred_element_type=jnp.float32
    )
    past = past * ratio_value + offsets[:, :, None, :]
    live = jnp.arange(cache_len, dtype=jnp.int32)[None, :] < length_row[:, None]
    past = jnp.where(live[:, None, None, :], past, -jnp.inf)
    self_part = (
        jnp.einsum(
            "rifs,ris->rif", query_grid_four, self_key_row, preferred_element_type=jnp.float32
        )
        * ratio_value
    )
    highest = jnp.maximum(jnp.max(past, axis=-1), self_part)
    past_exp = jnp.exp(past - highest[..., None])
    own_exp = jnp.exp(self_part - highest)
    denominator = jnp.sum(past_exp, axis=-1) + own_exp
    past_weight = (past_exp / denominator[..., None]).astype(jnp.bfloat16)
    own_weight = (own_exp / denominator).astype(jnp.bfloat16)
    mixed = jnp.einsum(
        "bkgl,blkd->bkgd", past_weight, value_four, preferred_element_type=jnp.float32
    )
    mixed = mixed + own_weight.astype(jnp.float32)[..., None] * own_value[:, :, None, :]
    return mixed.reshape(amount, queries.shape[1]).astype(jnp.bfloat16)


def local(
    tokens,
    cache_keys,
    cache_values,
    cum_gates,
    lengths,
    query_weight,
    key_weight,
    value_weight,
    forget_weight,
    out_weight,
    norm_gain,
    norm_bias,
    dense_gate_weight,
    dense_up_weight,
    dense_down_weight,
    dense_scale,
    expert_gate_weight,
    expert_up_weight,
    expert_down_weight,
    routes,
    route_weights,
):
    query = jnp.dot(tokens, query_weight, preferred_element_type=jnp.float32).astype(jnp.bfloat16)
    new_key = jnp.dot(tokens, key_weight, preferred_element_type=jnp.float32).astype(jnp.bfloat16)
    new_value = jnp.dot(tokens, value_weight, preferred_element_type=jnp.float32).astype(
        jnp.bfloat16
    )
    new_gate = jax.nn.log_sigmoid(
        jnp.dot(tokens, forget_weight, preferred_element_type=jnp.float32)
    )
    attended = attend(
        query, cache_keys, cache_values, cum_gates, lengths, new_key, new_value, new_gate
    )
    projected = jnp.dot(
        attended,
        lax.all_gather(out_weight, "ep", axis=0, tiled=True),
        preferred_element_type=jnp.float32,
    )
    settled = layer_norm(
        residual_scale * tokens.astype(jnp.float32) + projected, norm_gain[0], norm_bias[0]
    )
    return ffn_call(
        settled,
        jnp.transpose(routes),
        jnp.transpose(route_weights),
        jnp.transpose(expert_gate_weight),
        jnp.transpose(expert_up_weight),
        expert_down_weight,
        jnp.transpose(dense_gate_weight),
        jnp.transpose(dense_up_weight),
        dense_down_weight,
        dense_scale.reshape(1, -1),
        norm_gain,
        norm_bias,
    )


def solution(mesh):
    return jax.shard_map(
        local,
        mesh=mesh,
        in_specs=(
            P("ep", None),
            P("ep", None, None),
            P("ep", None, None),
            P("ep", None, None),
            P("ep"),
            P(),
            P(),
            P(),
            P(),
            P("ep", None),
            P(),
            P(),
            P(None, "ep"),
            P(None, "ep"),
            P("ep", None),
            P(),
            P(None, "ep"),
            P(None, "ep"),
            P("ep", None),
            P(),
            P(),
        ),
        out_specs=P("ep", None),
        check_vma=False,
    )
```

time: 265 us -> 150 us (0.57)
  waiting for transfers between devices: 135 us -> 56.8 us
  Pallas kernels: 0 us -> 53.5 us
  starting transfers between devices: 40.8 us -> 0.01 us
  matrix products: 29.7 us -> 11.2 us
  other arithmetic: 17.5 us -> 1.54 us
  local copies, waits for them, and re-layouts: 27.2 us -> 13.4 us
    ppermute x11 -> x0, waiting for transfers between devices: 75.8 us -> none  [partner_2(): return lax.ppermute(block, axis, route)]
    pallas_call x0 -> x1, Pallas kernels: none -> 53.5 us  [ffn_call(): pl.pallas_call(ffn_kernel, out_shape=jax.ShapeDtypeStruct((ROWS, WIDTH),...]
    all_to_all x2 -> x0, starting transfers between devices: 21.2 us -> none  [the longest x1 12.5 us: experts_by_exchange(): lax.all_to_all(outgoing, 'ep', split_axis=0, concat_axis=0, tiled=True)]
    ppermute x11 -> x0, starting transfers between devices: 19.6 us -> none  [partner_2(): return lax.ppermute(block, axis, route)]
    dot_general x6 -> x0, matrix products: 14.8 us -> none  [the longest x1 5.22 us: expert_part(): jnp.dot(hidden, down_rows, preferred_element_type=jnp.float32)]
    select_n x6 -> x0, other arithmetic: 11.1 us -> none  [the longest x3 11 us: local(): jnp.where(upper, jnp.concatenate([partner, stacked], axis=2), jnp.concate...]
    reshape x2 -> x0, local copies, waits for them, and re-layouts: 10.2 us -> none  [the longest x1 5.15 us: experts_by_exchange(): answered = result.reshape(received.shape)]
    all_to_all x2 -> x0, waiting for transfers between devices: 5.76 us -> none  [the longest x1 5.76 us: experts_by_exchange(): lax.all_to_all(answered, 'ep', split_axis=0, concat_axis=0, tiled=True)]
  transfers between devices with their start and end apart: 14 -> 1, of which waited for: 8 -> 1; matrix products, arithmetic and copies ran while one was open for 27% -> 12% of each run, Pallas kernels for 0% -> 0%
where the time goes in v1:
time: 150 us
  waiting for transfers between devices  56.8 us (38%)
  Pallas kernels  53.5 us (36%)
  between operations  13.6 us (9%)
  local copies, waits for them, and re-layouts  13.4 us (9%)
  matrix products  11.2 us (7%)
  other arithmetic  1.54 us (1%)
    all_gather x1, waiting for transfers between devices, local(): lax.all_gather(out_weight, 'ep', axis=0, tiled=True)  56 us
    pallas_call x1, Pallas kernels, ffn_call(): pl.pallas_call(ffn_kernel, out_shape=jax.ShapeDtypeStruct((ROWS, WIDTH),...  53.5 us
    unnamed x19, local copies, waits for them, and re-layouts  11.6 us
    dot_general x1, matrix products, local(): jnp.dot(attended, lax.all_gather(out_weight, 'ep', axis=0, tiled=True), p...  4.68 us
    dot_general x1, matrix products, local(): jnp.dot(tokens, query_weight, preferred_element_type=jnp.float32)  4.62 us
  transfers between devices with their start and end apart: 1, of which 1 were waited for; matrix products, arithmetic and copies ran while one was open for 12% of the time, Pallas kernels for 0%

profile of v1, /device:TPU:0, one launch (start us, length us, event | category | flops | bytes accessed | tf_op | source)
XLA Modules:
  0.0 149.9 jit_solution(12282740912473772604)
XLA Ops:
  6.5 0.7 all-gather.2.cloned.1.call-update
  7.3 4.6 %convolution_convert_fusion = bf16[8,2048]{1,0:T(8,128)(2,1)S(1)} fusion(bf16[8,2048]{1,0:T(8,128)(2,1)} %param.21, bf16[2048,2048]{1,0:T(8,128)(2,1)} %param.26), kind=kOutput, calls=%fused_computation.2 | convolution fusion | flops 67125248 | bytes 8454144 | tf_op jit(solution)/shard_map/dot_general | solution.py:376
  11.9 0.1 reshape.77
  12.0 0.0 copy-start.2
  12.1 0.0 copy-start.6
  12.1 2.6 %copy.27 = f32[8,1024,2]{2,1,0:T(8,128)} copy(f32[8,1024,2]{1,2,0:T(2,128)S(1)} %copy-done.4) | data formatting | bytes 131072 | tf_op args[3]
  14.7 0.2 fusion.8
  14.9 0.1 copy.28
  15.0 2.9 %copy.26 = bf16[8,1024,128]{1,2,0:T(8,128)(2,1)S(1)} copy(bf16[8,1024,128]{2,1,0:T(8,128)(2,1)} %param.22) | data formatting | bytes 4194304 | tf_op args[1]
  17.8 0.2 convolution_convert_fusion.2
  18.0 0.1 reshape.95
  18.1 4.0 %copy.29 = bf16[8,1024,128]{1,2,0:T(8,128)(2,1)} copy(bf16[8,1024,128]{2,1,0:T(8,128)(2,1)} %param.23) | data formatting | bytes 4194304 | tf_op args[2]
  22.1 0.2 fusion.3
  22.2 0.1 reshape.82
  22.4 1.3 gather_fusion
  23.6 0.1 iota_compare_fusion
  23.7 0.1 broadcast_select_fusion
  23.8 0.1 fusion.13
  23.9 0.1 add_bitcast_fusion
  24.0 0.5 fusion.11
  24.6 0.3 fusion.4
  24.9 0.7 copy-done.1
  25.6 0.7 fusion.2
  26.3 0.2 convert_element_type.39
  26.5 0.0 slice-start
  26.5 0.0 slice-start.1
  26.5 56.0 %all-gather.2.cloned.1.call-done = bf16[2048,2048]{1,0:T(8,128)(2,1)} async-done(((bf16[16,2048]{1,0:T(8,128)(2,1)}), bf16[2048,2048]{1,0:T(8,128)(2,1)}) %all-gather.2.cloned.1.call-update) | async-done | bytes 8388624 | tf_op jit(solution)/shard_map/all_gather | solution.py:389
  82.6 4.7 %fusion.12 = (f32[8]{0:T(128)S(1)}, f32[8,2048]{1,0:T(8,128)S(1)}) fusion(bf16[8,2048]{1,0:T(8,128)(2,1)S(1)} %convert_element_type.39, bf16[2048,2048]{1,0:T(8,128)(2,1)} %all-gather.2.cloned.1.call-done, bf16[8,2048]{1,0:T(8,128)(2,1)S(1)} %copy-done.2), kind=kOutput, calls=%fused_computation.37 | convolution fusion | flops 67174392 | bytes 8519712 | tf_op jit(solution)/shard_map/dot_general | solution.py:387
  87.3 0.2 multiply_reduce_fusion
  87.5 0.7 add_convert_fusion.settled_ref
  88.2 53.5 %ffn.1 = bf16[8,2048]{1,0:T(8,128)(2,1)} custom-call(bf16[8,2048]{1,0:T(8,128)(2,1)} %add_convert_fusion.settled_ref, s32[2,1024]{1,0:T(2,128)} %bitcast.48, f32[2,1024]{1,0:T(2,128)} %bitcast.49, bf16[448,2048]{1,0:T(8,128)(2,1)} %bitcast.40, bf16[448,2048]{1,0:T(8,128)(2,1)} %bitcast.41, bf16[448,2048]{1,0:T(8,128)(2,1)} %down_hbm.1, ...), custom_call_target="tpu_custom_call" | custom-call | tf_op jit(solution)/shard_map/ffn/pallas_call | solution.py:276
  141.7 1.4 copy.33
  (23 shorter events, 0.1 us)
Async XLA Ops:
  6.5 11.3 %copy-start = (bf16[2048,128]{1,0:T(8,128)(2,1)S(1)}, bf16[2048,128]{1,0:T(8,128)(2,1)}, u32[]{:S(2)}) copy-start(bf16[2048,128]{1,0:T(8,128)(2,1)} %param.27) | copy-start | bytes 1572868
  6.5 76.0 %all-gather.2.cloned.1.call-start = ((), (), s32[]{:S(2)}) async-start(), calls=%async_computation | async-start | bytes 8454144 | tf_op jit(solution)/shard_map/all_gather | solution.py:389
  7.3 4.8 %copy-start.4 = (f32[8,1024,2]{1,2,0:T(2,128)S(1)}, f32[8,1024,2]{1,2,0:T(2,128)}, u32[]{:S(2)}) copy-start(f32[8,1024,2]{1,2,0:T(2,128)} %param.24) | copy-start | bytes 196612
  12.0 2.7 %copy-start.2 = (bf16[8,2048]{1,0:T(8,128)(2,1)S(1)}, bf16[8,2048]{1,0:T(8,128)(2,1)}, u32[]{:S(2)}) copy-start(bf16[8,2048]{1,0:T(8,128)(2,1)} %param.21) | copy-start | bytes 98308
  12.1 2.7 %copy-start.6 = (bf16[2048,2]{0,1:T(2,128)(2,1)S(1)}, bf16[2048,2]{0,1:T(2,128)(2,1)}, u32[]{:S(2)}) copy-start(bf16[2048,2]{0,1:T(2,128)(2,1)} %param.29) | copy-start | bytes 24580
  18.1 4.0 %copy-start.3 = (bf16[2048,128]{1,0:T(8,128)(2,1)S(1)}, bf16[2048,128]{1,0:T(8,128)(2,1)}, u32[]{:S(2)}) copy-start(bf16[2048,128]{1,0:T(8,128)(2,1)} %param.28) | copy-start | bytes 1572868
  18.1 4.2 %copy-start.5 = (s32[8]{0:T(128)S(1)}, s32[8]{0:T(128)}, u32[]{:S(2)}) copy-start(s32[8]{0:T(128)} %param.25) | copy-start | bytes 100
  24.0 1.6 %copy-start.1 = (bf16[8,1024,128]{1,2,0:T(8,128)(2,1)S(1)}, bf16[8,1024,128]{1,2,0:T(8,128)(2,1)}, u32[]{:S(2)}) copy-start(bf16[8,1024,128]{1,2,0:T(8,128)(2,1)} %copy.29) | copy-start | bytes 6291460
  26.5 61.0 %slice-start = ((f32[2,2048]{1,0:T(2,128)}), f32[1,2048]{1,0:T(1,128)S(1)}, s32[]{:S(2)}) async-start(f32[2,2048]{1,0:T(2,128)} %bias_ref.1), calls=%async_computation.1 | async-start | bytes 16384 | tf_op jit(solution)/shard_map/slice | solution.py:393
  26.5 61.0 %slice-start.1 = ((f32[2,2048]{1,0:T(2,128)}), f32[1,2048]{1,0:T(1,128)S(1)}, s32[]{:S(2)}) async-start(f32[2,2048]{1,0:T(2,128)} %gain_ref.1), calls=%async_computation.2 | async-start | bytes 16384 | tf_op jit(solution)/shard_map/slice | solution.py:393
Sparse Core Ops, SparseCore 0:
  10.3 72.2 all-gather.1

commit v2 on v1

--- a/solution.py
+++ b/solution.py
@@ -19,6 +19,7 @@
 FFP = 512
 CHUNKS = ((0, 768), (768, 640), (1408, 640))
 GATHER_ORDER = ((2, 1, 0), (0, 2, 1), (1, 0, 2))
+ATTEND = 4
 residual_scale = 1.4142135
 norm_eps = 1e-05
 
@@ -148,22 +149,254 @@
     return [d for d in range(3) if d not in gone]
 
 
-def ffn_kernel(
-    settled_ref, routes_ref, shares_ref, gate_hbm, up_hbm, down_hbm, dgate_ref, dup_ref, ddown_ref,
+PROJ = 512
+HALF = 256
+WEIGHT_ORDER = ((1, 0), (0, 1))
+NT = (((1,), (1,)), ((), ()))
+GROUP = 4
+HEAD_LANES = 64
+
+
+def weight_region(wo_ref, k, core, spot, done):
+    where = tuple(pl.ds(0, SIDE) if d in done else spot[d] for d in range(2))
+    return wo_ref.at[where + (pl.ds(0, SIDE), core, pl.ds(0, 2 * ROWS), pl.ds(k * HALF, HALF))]
+
+
+class WeightGather:
+    def __init__(self, ow_hbm, wo_ref, core, spot, own, wsend, wrecv, xsend, xrecv, fsend, frecv, hsend, hrecv):
+        self.ow, self.wo, self.core, self.spot, self.own = ow_hbm, wo_ref, core, spot, own
+        self.wsend, self.wrecv, self.xsend, self.xrecv = wsend, wrecv, xsend, xrecv
+        self.fsend, self.frecv, self.hsend, self.hrecv = fsend, frecv, hsend, hrecv
+        self.partner = device_at(1 - core, spot)
+        self.started = []
+
+    def go(self, copy):
+        copy.start()
+        self.started.append(copy)
+
+    def line_copy(self, offset, source, target):
+        z, y, x = source
+        first = pl.multiple_of(target[2] * PROJ, PROJ)
+        return remote(
+            self.ow.at[:, pl.ds(first, PROJ)], self.wo.at[z, y, x, self.core],
+            self.xsend.at[offset - 1], self.xrecv.at[offset - 1], device_at(self.core, target),
+        )
+
+    def own_copy(self):
+        z, y, x = self.spot
+        first = pl.multiple_of(x * PROJ, PROJ)
+        return pltpu.make_async_copy(self.ow.at[:, pl.ds(first, PROJ)], self.wo.at[z, y, x, self.core], self.own)
+
+    def line_start(self):
+        self.own_copy().start()
+        for offset in range(1, SIDE):
+            self.go(self.line_copy(offset, self.spot, shifted(self.spot, 2, offset)))
+
+    def line_arrive(self):
+        self.own_copy().wait()
+        for offset in range(1, SIDE):
+            self.line_copy(offset, shifted(self.spot, 2, -offset), self.spot).wait_recv()
+        self.go(self.line_forward(self.core))
+
+    def line_forward(self, core):
+        z, y, x = self.spot
+        region = self.wo.at[z, y, pl.ds(0, SIDE), core]
+        return remote(region, region, self.hsend, self.hrecv, self.partner)
+
+    def copy(self, k, phase, offset, source, target):
+        region = weight_region(self.wo, k, self.core, source, WEIGHT_ORDER[k][:phase])
+        return remote(
+            region, region, self.wsend.at[k, phase, offset - 1], self.wrecv.at[k, phase, offset - 1],
+            device_at(self.core, target),
+        )
+
+    def start(self, phase):
+        for k in range(2):
+            for offset in range(1, SIDE):
+                target = shifted(self.spot, WEIGHT_ORDER[k][phase], offset)
+                self.go(self.copy(k, phase, offset, self.spot, target))
+
+    def forward_copy(self, k, phase, offset, core):
+        source = shifted(self.spot, WEIGHT_ORDER[k][phase], -offset)
+        region = weight_region(self.wo, k, core, source, WEIGHT_ORDER[k][:phase])
+        return remote(
+            region, region, self.fsend.at[k, phase, offset - 1], self.frecv.at[k, phase, offset - 1], self.partner
+        )
+
+    def arrive(self, phase):
+        for k in range(2):
+            for offset in range(1, SIDE):
+                source = shifted(self.spot, WEIGHT_ORDER[k][phase], -offset)
+                self.copy(k, phase, offset, source, self.spot).wait_recv()
+
+    def forward(self, phase):
+        for k in range(2):
+            for offset in range(1, SIDE):
+                self.go(self.forward_copy(k, phase, offset, self.core))
+
+    def finish(self):
+        self.line_forward(1 - self.core).wait_recv()
+        for phase in range(2):
+            for k in range(2):
+                for offset in range(1, SIDE):
+                    self.forward_copy(k, phase, offset, 1 - self.core).wait_recv()
+
+
+def spread_heads(pairs):
+    lane = lax.broadcasted_iota(jnp.int32, (8, 2 * HEAD_LANES), 1)
+    low = lane < HEAD_LANES
+    first, second = pairs[:8], pairs[8:]
+    return jnp.concatenate(
+        [
+            jnp.where(low, first, 0.0),
+            jnp.where(low, pltpu.roll(first, HEAD_LANES, 1), 0.0),
+            jnp.where(low, 0.0, pltpu.roll(second, HEAD_LANES, 1)),
+            jnp.where(low, 0.0, second),
+        ],
+        axis=0,
+    )
+
+
+def pair_heads(heads):
+    lane = lax.broadcasted_iota(jnp.int32, (8, 2 * HEAD_LANES), 1)
+    low = lane < HEAD_LANES
+    first = jnp.where(low, heads[:8], pltpu.roll(heads[8:16], HEAD_LANES, 1))
+    second = jnp.where(low, pltpu.roll(heads[16:24], HEAD_LANES, 1), heads[24:])
+    return jnp.concatenate([first, second], axis=0)
+
+
+def attend_some(first, count, lengths_ref, keys_ref, values_ref, gates_ref, pairs_ref, fresh_ref, gate_ref, mixed_ref):
+    slots = keys_ref.shape[1]
+    place = lax.broadcasted_iota(jnp.int32, (2, slots), 1)
+    column = lax.broadcasted_iota(jnp.int32, (2, ROWS), 1)
+    state = []
+    for step in range(count):
+        b = first + step
+        queries = spread_heads(pairs_ref[b])
+        scores = lax.dot_general(
+            queries.astype(BF16), keys_ref[b], NT, preferred_element_type=F32
+        )
+        length = lengths_ref[b]
+        sums = gates_ref[b]
+        latest = jnp.sum(jnp.where(place == length - 1, sums, 0.0), axis=1, keepdims=True)
+        fresh_gate = jnp.sum(jnp.where(column == b, gate_ref[...], 0.0), axis=1, keepdims=True)
+        offsets = jnp.where(place < length, latest - sums + fresh_gate, -jnp.inf)
+        wide = jnp.concatenate(
+            [jnp.broadcast_to(offsets[:1], (16, slots)), jnp.broadcast_to(offsets[1:], (16, slots))], axis=0
+        )
+        scores = scores + wide
+        fresh = fresh_ref[pl.ds(b, 1), :]
+        own = jnp.sum(queries * fresh[:, : 2 * HEAD_LANES], axis=1, keepdims=True)
+        state.append((scores, own, fresh[:, 2 * HEAD_LANES :]))
+    for step, (scores, own, fresh_value) in enumerate(state):
+        b = first + step
+        highest = jnp.maximum(jnp.max(scores, axis=1, keepdims=True), own)
+        past = jnp.exp(scores - highest)
+        own = jnp.exp(own - highest)
+        ratio = 1.0 / (jnp.sum(past, axis=1, keepdims=True) + own)
+        weights = (past * ratio).astype(BF16)
+        own_weight = (own * ratio).astype(BF16).astype(F32)
+        mixed = jnp.dot(weights, values_ref[b], preferred_element_type=F32) + own_weight * fresh_value
+        mixed_ref[b] = pair_heads(mixed)
+
+
+def step_kernel(
+    lengths_ref, tokens_hbm, keys_hbm, values_hbm, gates_hbm, query_hbm, key_hbm, value_hbm, forget_hbm, ow_hbm,
+    routes_hbm, shares_hbm, gate_hbm, up_hbm, down_hbm, dgate_ref, dup_ref, ddown_ref,
     scale_ref, gain_ref, bias_ref, out_ref,
+    tokens_ref, keys_ref, values_ref, gates_ref, wq_ref, wkv_ref, forget_ref, wo_ref, routes_ref, shares_ref,
+    pairs_ref, mixed_ref, fresh_ref, newgate_ref, line_ref, sent_ref, back_ref, settled_ref,
     rows_ref, wg_ref, wu_ref, wd_ref, factor_ref, part_ref, twin_ref, r0_ref, r1_ref, r2_ref, s1_ref, s2_ref,
-    wsem, gsend, grecv, fsend, frecv, osend, orecv, tsend, trecv, rsend, rrecv,
+    wsem, asem, owsem, wxsend, wxrecv, wwsend, wwrecv, wfsend, wfrecv, whsend, whrecv,
+    lsend, lrecv, bsend, brecv,
+    gsend, grecv, fsend, frecv, osend, orecv, tsend, trecv, rsend, rrecv,
 ):
     core, spot = position()
-    entry_barrier(core, spot)
+    depth = WIDTH // GROUP
+    small = [
+        pltpu.make_async_copy(tokens_hbm, tokens_ref, asem.at[0]),
+        pltpu.make_async_copy(forget_hbm, forget_ref, asem.at[1]),
+        pltpu.make_async_copy(key_hbm, wkv_ref.at[:, pl.ds(0, 128)], asem.at[2]),
+        pltpu.make_async_copy(value_hbm, wkv_ref.at[:, pl.ds(128, 128)], asem.at[3]),
+    ]
+    wide = [
+        pltpu.make_async_copy(
+            query_hbm.at[pl.ds(i * depth, depth)], wq_ref.at[pl.ds(i * depth, depth)], asem.at[4 + i]
+        )
+        for i in range(GROUP)
+    ]
+    cache = [
+        pltpu.make_async_copy(keys_hbm, keys_ref, asem.at[8]),
+        pltpu.make_async_copy(values_hbm, values_ref, asem.at[9]),
+        pltpu.make_async_copy(gates_hbm, gates_ref, asem.at[10]),
+    ]
     loads = [
         pltpu.make_async_copy(gate_hbm, wg_ref.at[pl.ds(0, FFE)], wsem.at[0]),
         pltpu.make_async_copy(up_hbm, wu_ref.at[pl.ds(0, FFE)], wsem.at[1]),
         pltpu.make_async_copy(down_hbm, wd_ref.at[pl.ds(0, FFE)], wsem.at[2]),
+        pltpu.make_async_copy(routes_hbm, routes_ref, wsem.at[3]),
+        pltpu.make_async_copy(shares_hbm, shares_ref, wsem.at[4]),
     ]
+    for load in small + wide:
+        load.start()
+    entry_barrier(core, spot)
+    weights = WeightGather(
+        ow_hbm, wo_ref, core, spot, owsem, wwsend, wwrecv, wxsend, wxrecv, wfsend, wfrecv, whsend, whrecv
+    )
+    weights.line_start()
+    for load in cache + loads:
+        load.start()
+
+    for load in small:
+        load.wait()
+    tokens = tokens_ref[...]
+    fresh_ref[...] = jnp.dot(tokens, wkv_ref[...], preferred_element_type=F32).astype(BF16).astype(F32)
+    raw = lax.dot_general(forget_ref[...], tokens, NT, preferred_element_type=F32)
+    newgate_ref[...] = jnp.minimum(raw, 0.0) - jnp.log1p(jnp.exp(-jnp.abs(raw)))
+    query = jnp.zeros((ROWS, WIDTH), F32)
+    for i in range(GROUP):
+        wide[i].wait()
+        query = query + jnp.dot(
+            tokens[:, i * depth : (i + 1) * depth], wq_ref[i * depth : (i + 1) * depth, :], preferred_element_type=F32
+        )
+    query = query.astype(BF16).astype(F32) * HEAD_LANES**-0.5
+    flat = pairs_ref.reshape(ROWS * 16, 128)
+    for i in range(16):
+        flat[pl.ds(i, ROWS, stride=16), :] = query[:, 128 * i : 128 * (i + 1)]
+    weights.line_arrive()
+    weights.start(0)
+    for load in cache:
+        load.wait()
+
+    def some(i, carry):
+        attend_some(
+            i * ATTEND, ATTEND, lengths_ref, keys_ref, values_ref, gates_ref, pairs_ref, fresh_ref, newgate_ref,
+            mixed_ref,
+        )
+        return carry
+
+    turns = ROWS // ATTEND
+    lax.fori_loop(0, turns // 2, some, 0)
+    weights.arrive(0)
+    weights.start(1)
+    weights.forward(0)
+    lax.fori_loop(turns // 2, turns, some, 0)
+
+    flat = mixed_ref.reshape(ROWS * 16, 128)
+    attended = jnp.concatenate([flat[pl.ds(i, ROWS, stride=16), :] for i in range(16)], axis=1).astype(BF16)
+    line_ref[spot[2]] = attended
+
+    def line_copy(offset, source, target):
+        return remote(
+            line_ref.at[source[2]], line_ref.at[source[2]], lsend.at[offset - 1], lrecv.at[offset - 1],
+            device_at(core, target),
+        )
+
+    for offset in range(1, SIDE):
+        weights.go(line_copy(offset, spot, shifted(spot, 2, offset)))
+
     for load in loads:
-        load.start()
-    rows_ref[(core,) + spot] = settled_ref[...]
+        load.wait()
     pad = jnp.zeros((FFP - FFE - FFD, WIDTH), BF16)
     for ref, dense in ((wg_ref, dgate_ref[...]), (wu_ref, dup_ref[...])):
         ref[FFE:, :] = jnp.concatenate([dense, pad], axis=0)
@@ -175,18 +408,41 @@
     turned = jnp.transpose(jnp.broadcast_to(factor, (8, factor.shape[1])))
     factor_ref[...] = turned.reshape(factor_ref.shape)
 
+    weights.arrive(1)
+    weights.forward(1)
+    for offset in range(1, SIDE):
+        line_copy(offset, shifted(spot, 2, -offset), spot).wait_recv()
+    weights.finish()
+    lines = line_ref.reshape(SIDE * ROWS, WIDTH)[...]
+    sent_ref.reshape(SIDE * ROWS, PROJ)[...] = jnp.dot(
+        lines, wo_ref.reshape(WIDTH, PROJ)[...], preferred_element_type=F32
+    )
+
+    def back_copy(offset, source, target):
+        return remote(
+            sent_ref.at[target[2]], back_ref.at[source[2]], bsend.at[offset - 1], brecv.at[offset - 1],
+            device_at(core, target),
+        )
+
+    for offset in range(1, SIDE):
+        weights.go(back_copy(offset, spot, shifted(spot, 2, offset)))
+    back_ref[spot[2]] = sent_ref[spot[2]]
+    for offset in range(1, SIDE):
+        back_copy(offset, shifted(spot, 2, -offset), spot).wait_recv()
+    projected = jnp.concatenate([back_ref[i] for i in range(SIDE)], axis=1)
+    settled = norm_rows(residual_scale * tokens.astype(F32) + projected, gain_ref[0:1, :], bias_ref[0:1, :])
+    settled_ref[...] = settled
+    rows_ref[(core,) + spot] = settled
+
     started = gather_rows(rows_ref, core, spot, gsend, grecv, fsend, frecv, osend, orecv)
-    for load in loads:
-        load.wait()
-
-    nt = (((1,), (1,)), ((), ()))
+
     block = 2 * SIDE * SIDE * ROWS
     lane = lax.broadcasted_iota(jnp.int32, (1, FFP), 1)
 
     def part_of(half, plane):
         x = rows_ref.at[half, pl.ds(plane, 2)].reshape(block, WIDTH)[...]
-        gate = lax.dot_general(x, wg_ref[...], nt, preferred_element_type=F32)
-        up = lax.dot_general(x, wu_ref[...], nt, preferred_element_type=F32)
+        gate = lax.dot_general(x, wg_ref[...], NT, preferred_element_type=F32)
+        up = lax.dot_general(x, wu_ref[...], NT, preferred_element_type=F32)
         weight = factor_ref[pl.ds(plane * SIDE * SIDE, 2 * SIDE * SIDE), half].reshape(block, 8)[:, :1]
         weight = jnp.where(lane < FFE, weight, 1.0)
         hidden = (gate * jax.nn.sigmoid(gate) * up * weight).astype(BF16)
@@ -262,23 +518,43 @@
     out_ref[...] = norm_rows(
         residual_scale * settled_ref[...].astype(F32) + ffn, gain_ref[1:2, :], bias_ref[1:2, :]
     )
-    for copy in started:
+    for copy in weights.started + started:
         copy.wait_send()
     for i in range(SIDE // 2):
         twin_copy(i).wait_send()
 
 
-def ffn_call(settled, routes, shares, gate, up, down, dgate, dup, ddown, scale, gain, bias):
+def step_call(lengths, *operands):
     vmem = pl.BlockSpec(memory_space=pltpu.VMEM)
     hbm = pl.BlockSpec(memory_space=pltpu.HBM)
     sem = pltpu.SemaphoreType.DMA
     cube = (SIDE, SIDE, SIDE, ROWS, WIDTH)
+    slots = operands[1].shape[1]
+    peers = SIDE - 1
     return pl.pallas_call(
-        ffn_kernel,
+        step_kernel,
         out_shape=jax.ShapeDtypeStruct((ROWS, WIDTH), BF16),
-        in_specs=[vmem, vmem, vmem, hbm, hbm, hbm, vmem, vmem, vmem, vmem, vmem, vmem],
+        in_specs=[pl.BlockSpec(memory_space=pltpu.SMEM)] + [hbm] * 14 + [vmem] * 6,
         out_specs=vmem,
         scratch_shapes=[
+            pltpu.VMEM((ROWS, WIDTH), BF16),
+            pltpu.VMEM((ROWS, slots, 128), BF16),
+            pltpu.VMEM((ROWS, slots, 128), BF16),
+            pltpu.VMEM((ROWS, 2, slots), F32),
+            pltpu.VMEM((WIDTH, WIDTH), BF16),
+            pltpu.VMEM((WIDTH, 256), BF16),
+            pltpu.VMEM((2, WIDTH), BF16),
+            pltpu.VMEM((SIDE, SIDE, SIDE, 2, 2 * ROWS, PROJ), BF16),
+            pltpu.VMEM((2, 2 * SIDE**3 * ROWS), jnp.int32),
+            pltpu.VMEM((2, 2 * SIDE**3 * ROWS), F32),
+            pltpu.VMEM((ROWS, 16, 128), F32),
+            pltpu.VMEM((ROWS, 16, 128), F32),
+            pltpu.VMEM((ROWS, 256), F32),
+            pltpu.VMEM((2, ROWS), F32),
+            pltpu.VMEM((SIDE, ROWS, WIDTH), BF16),
+            pltpu.VMEM((SIDE, ROWS, PROJ), F32),
+            pltpu.VMEM((SIDE, ROWS, PROJ), F32),
+            pltpu.VMEM((ROWS, WIDTH), BF16),
             pltpu.VMEM((2,) + cube, BF16),
             pltpu.VMEM((FFP, WIDTH), BF16),
             pltpu.VMEM((FFP, WIDTH), BF16),
@@ -286,68 +562,28 @@
             pltpu.VMEM((SIDE**3, 2, ROWS, 8), F32),
             pltpu.VMEM((2,) + cube, BF16),
             pltpu.VMEM(cube, BF16),
-            pltpu.VMEM((SIDE - 1,) + cube[1:], BF16),
-            pltpu.VMEM((SIDE - 1,) + cube[2:], BF16),
-            pltpu.VMEM((SIDE - 1,) + cube[3:], BF16),
+            pltpu.VMEM((peers,) + cube[1:], BF16),
+            pltpu.VMEM((peers,) + cube[2:], BF16),
+            pltpu.VMEM((peers,) + cube[3:], BF16),
             pltpu.VMEM(cube[1:], BF16),
             pltpu.VMEM(cube[2:], BF16),
-            sem((3,)),
-            sem((3, 3, SIDE - 1)), sem((3, 3, SIDE - 1)),
-            sem((3, 3, SIDE - 1)), sem((3, 3, SIDE - 1)),
+            sem((5,)), sem((11,)), sem,
+            sem((peers,)), sem((peers,)),
+            sem((2, 2, peers)), sem((2, 2, peers)),
+            sem((2, 2, peers)), sem((2, 2, peers)),
+            sem, sem,
+            sem((peers,)), sem((peers,)), sem((peers,)), sem((peers,)),
+            sem((3, 3, peers)), sem((3, 3, peers)),
+            sem((3, 3, peers)), sem((3, 3, peers)),
             sem, sem,
             sem((SIDE // 2,)), sem((SIDE // 2,)),
-            sem((3, 3, SIDE - 1)), sem((3, 3, SIDE - 1)),
+            sem((3, 3, peers)), sem((3, 3, peers)),
         ],
         compiler_params=pltpu.CompilerParams(
             collective_id=0, has_side_effects=True, vmem_limit_bytes=60 * 2**20
         ),
-        name="ffn",
-    )(settled, routes, shares, gate, up, down, dgate, dup, ddown, scale, gain, bias)
-
-
-def layer_norm(values, gain_row, shift_row):
-    return norm_rows(values, gain_row, shift_row)
-
-
-def attend(
-    queries, cached_keys, cached_values, gate_sums, length_row, fresh_key, fresh_value, fresh_gate
-):
-    amount = queries.shape[0]
-    cache_len = cached_keys.shape[1]
-    kv_count = fresh_gate.shape[1]
-    head_dim = fresh_key.shape[1] // kv_count
-    grouped = queries.shape[1] // (kv_count * head_dim)
-    query_grid_four = queries.reshape(amount, kv_count, grouped, head_dim)
-    key_four = cached_keys.reshape(amount, cache_len, kv_count, head_dim)
-    value_four = cached_values.reshape(amount, cache_len, kv_count, head_dim)
-    self_key_row = fresh_key.reshape(amount, kv_count, head_dim)
-    own_value = fresh_value.astype(jnp.float32).reshape(amount, kv_count, head_dim)
-    ratio_value = head_dim ** (-0.5)
-    latest = jnp.take_along_axis(gate_sums, (length_row - 1)[:, None, None], axis=1)
-    offsets = jnp.transpose(latest - gate_sums + fresh_gate[:, None, :], (0, 2, 1))
-    past = jnp.einsum(
-        "bkgd,blkd->bkgl", query_grid_four, key_four, preferred_element_type=jnp.float32
-    )
-    past = past * ratio_value + offsets[:, :, None, :]
-    live = jnp.arange(cache_len, dtype=jnp.int32)[None, :] < length_row[:, None]
-    past = jnp.where(live[:, None, None, :], past, -jnp.inf)
-    self_part = (
-        jnp.einsum(
-            "rifs,ris->rif", query_grid_four, self_key_row, preferred_element_type=jnp.float32
-        )
-        * ratio_value
-    )
-    highest = jnp.maximum(jnp.max(past, axis=-1), self_part)
-    past_exp = jnp.exp(past - highest[..., None])
-    own_exp = jnp.exp(self_part - highest)
-    denominator = jnp.sum(past_exp, axis=-1) + own_exp
-    past_weight = (past_exp / denominator[..., None]).astype(jnp.bfloat16)
-    own_weight = (own_exp / denominator).astype(jnp.bfloat16)
-    mixed = jnp.einsum(
-        "bkgl,blkd->bkgd", past_weight, value_four, preferred_element_type=jnp.float32
-    )
-    mixed = mixed + own_weight.astype(jnp.float32)[..., None] * own_value[:, :, None, :]
-    return mixed.reshape(amount, queries.shape[1]).astype(jnp.bfloat16)
+        name="step",
+    )(lengths, *operands)
 
 
 def local(
@@ -373,27 +609,17 @@
     routes,
     route_weights,
 ):
-    query = jnp.dot(tokens, query_weight, preferred_element_type=jnp.float32).astype(jnp.bfloat16)
-    new_key = jnp.dot(tokens, key_weight, preferred_element_type=jnp.float32).astype(jnp.bfloat16)
-    new_value = jnp.dot(tokens, value_weight, preferred_element_type=jnp.float32).astype(
-        jnp.bfloat16
-    )
-    new_gate = jax.nn.log_sigmoid(
-        jnp.dot(tokens, forget_weight, preferred_element_type=jnp.float32)
-    )
-    attended = attend(
-        query, cache_keys, cache_values, cum_gates, lengths, new_key, new_value, new_gate
-    )
-    projected = jnp.dot(
-        attended,
-        lax.all_gather(out_weight, "ep", axis=0, tiled=True),
-        preferred_element_type=jnp.float32,
-    )
-    settled = layer_norm(
-        residual_scale * tokens.astype(jnp.float32) + projected, norm_gain[0], norm_bias[0]
-    )
-    return ffn_call(
-        settled,
+    return step_call(
+        lengths,
+        tokens,
+        cache_keys,
+        cache_values,
+        jnp.transpose(cum_gates, (0, 2, 1)),
+        query_weight,
+        key_weight,
+        value_weight,
+        jnp.transpose(forget_weight),
+        out_weight,
         jnp.transpose(routes),
         jnp.transpose(route_weights),
         jnp.transpose(expert_gate_weight),

time: 150 us -> 82.8 us (0.55)
  waiting for transfers between devices: 56.8 us -> 0 us
  Pallas kernels: 53.5 us -> 81.3 us
  between operations: 13.6 us -> 0.01 us
  local copies, waits for them, and re-layouts: 13.4 us -> 1.38 us
  matrix products: 11.2 us -> 0 us
  other arithmetic: 1.54 us -> 0 us
    all_gather x1 -> x0, waiting for transfers between devices: 56 us -> none  [local(): lax.all_gather(out_weight, 'ep', axis=0, tiled=True)]
    pallas_call x1, Pallas kernels: 53.5 us -> 81.3 us  [step_call(): pl.pallas_call(step_kernel, out_shape=jax.ShapeDtypeStruct((ROWS, WIDTH),...]
    dot_general x8 -> x0, matrix products: 11.2 us -> none  [the longest x1 4.68 us: local(): jnp.dot(attended, lax.all_gather(out_weight, 'ep', axis=0, tiled=True), p...]
    unnamed x19 -> x1, local copies, waits for them, and re-layouts: 11.6 us -> 1.38 us
  transfers between devices with their start and end apart: 1 -> 0, of which waited for: 1 -> 0; matrix products, arithmetic and copies ran while one was open for 12% -> 0% of each run, Pallas kernels for 0% -> 0%
where the time goes in v2:
time: 82.8 us; the launch traced here: 82.7 us
  Pallas kernels  81.3 us (98%)
  local copies, waits for them, and re-layouts  1.38 us (2%)
    pallas_call x1, Pallas kernels, step_call(): pl.pallas_call(step_kernel, out_shape=jax.ShapeDtypeStruct((ROWS, WIDTH),...  81.3 us

profile of v2, /device:TPU:0, one launch (start us, length us, event | category | flops | bytes accessed | tf_op | source)
XLA Modules:
  0.0 82.7 jit_solution(14461413942113426021)
XLA Ops:
  0.0 81.3 %step.1 = bf16[8,2048]{1,0:T(8,128)(2,1)} custom-call(s32[8]{0:T(128)} %lengths_ref.1, bf16[8,2048]{1,0:T(8,128)(2,1)} %tokens_hbm.1, bf16[8,1024,128]{2,1,0:T(8,128)(2,1)} %keys_hbm.1, bf16[8,1024,128]{2,1,0:T(8,128)(2,1)} %values_hbm.1, f32[8,2,1024]{2,1,0:T(2,128)} %bitcast.13, bf16[2048,2048]{1,0:T(8,128)(2,1)} %query_hbm.1, bf16[2048,128]{1,0:T(8,128)(2,1)} %key_hbm.1, ...), custom_call_target="tpu_custom_call" | custom-call | tf_op jit(solution)/shard_map/step/pallas_call | solution.py:534
  81.3 1.4 %copy.23 = bf16[8,2048]{1,0:T(8,128)(2,1)} copy(bf16[8,2048]{1,0:T(8,128)(2,1)} %step.1) | data formatting | bytes 65536

commit v3 on v2

v3 whole, which is shorter than its diff:
```python
import functools

import jax
import jax.numpy as jnp
from jax import lax
from jax.experimental import pallas as pl
from jax.experimental.pallas import tpu as pltpu
from jax.sharding import PartitionSpec as P

MESH = pl.DeviceIdType.MESH
F32 = jnp.float32
BF16 = jnp.bfloat16
SIDE = 4
ROWS = 8
WIDTH = 2048
EXPERTS = 8
FFE = 448
FFD = 44
FFP = 512
CHUNKS = ((0, 768), (768, 640), (1408, 640))
GATHER_ORDER = ((2, 1, 0), (0, 2, 1), (1, 0, 2))
ATTEND = 4
residual_scale = 1.4142135
norm_eps = 1e-05


def norm_rows(values, gain_row, shift_row):
    centre = jnp.mean(values, axis=-1, keepdims=True)
    centred = values - centre
    spread = jnp.mean(centred * centred, axis=-1, keepdims=True)
    return (centred * lax.rsqrt(spread + norm_eps) * gain_row + shift_row).astype(BF16)


def position():
    me = lax.axis_index("ep")
    core = me % 2
    x = (me // 2) % SIDE
    y = (me // (2 * SIDE)) % SIDE
    z = me // (2 * SIDE * SIDE)
    return core, (z, y, x)


def device_at(core, spot):
    z, y, x = spot
    return (((z * SIDE + y) * SIDE + x) * 2 + core,)


def moved(spot, dim, value):
    return tuple(value if d == dim else spot[d] for d in range(3))


def shifted(spot, dim, offset):
    return moved(spot, dim, (spot[dim] + offset + SIDE) % SIDE)


def columns(k):
    return pl.ds(CHUNKS[k][0], CHUNKS[k][1])


def remote(src, dst, send, recv, target):
    return pltpu.make_async_remote_copy(
        src_ref=src, dst_ref=dst, send_sem=send, recv_sem=recv, device_id=target, device_id_type=MESH
    )


def entry_signal(core, spot):
    barrier = pltpu.get_barrier_semaphore()
    for offset in range(SIDE):
        pl.semaphore_signal(
            barrier, inc=1, device_id=device_at(1 - core, shifted(spot, 2, offset)), device_id_type=MESH
        )
    for dim in range(3):
        for offset in range(1, SIDE):
            pl.semaphore_signal(
                barrier, inc=1, device_id=device_at(core, shifted(spot, dim, offset)), device_id_type=MESH
            )


def entry_wait():
    pl.semaphore_wait(pltpu.get_barrier_semaphore(), 3 * (SIDE - 1) + SIDE)


PROJ = 256
HALF = 128
WEIGHT_ORDER = ((1, 0), (0, 1))
NT = (((1,), (1,)), ((), ()))
GROUP = 4
HEAD_LANES = 64
PEERS = SIDE - 1
PIECES = (1, 3, 2)
LINE = tuple((offset, flip) for offset in range(SIDE) for flip in range(2))[1:]


def spread_heads(pairs):
    lane = lax.broadcasted_iota(jnp.int32, (8, 2 * HEAD_LANES), 1)
    low = lane < HEAD_LANES
    first, second = pairs[:8], pairs[8:]
    return jnp.concatenate(
        [
            jnp.where(low, first, 0.0),
            jnp.where(low, pltpu.roll(first, HEAD_LANES, 1), 0.0),
            jnp.where(low, 0.0, pltpu.roll(second, HEAD_LANES, 1)),
            jnp.where(low, 0.0, second),
        ],
        axis=0,
    )


def pair_heads(heads):
    lane = lax.broadcasted_iota(jnp.int32, (8, 2 * HEAD_LANES), 1)
    low = lane < HEAD_LANES
    first = jnp.where(low, heads[:8], pltpu.roll(heads[8:16], HEAD_LANES, 1))
    second = jnp.where(low, pltpu.roll(heads[16:24], HEAD_LANES, 1), heads[24:])
    return jnp.concatenate([first, second], axis=0)


def attend_some(first, count, lengths_ref, keys_ref, values_ref, gates_ref, pairs_ref, fresh_ref, gate_ref, mixed_ref):
    slots = keys_ref.shape[1]
    place = lax.broadcasted_iota(jnp.int32, (2, slots), 1)
    column = lax.broadcasted_iota(jnp.int32, (2, ROWS), 1)
    state = []
    for step in range(count):
        b = first + step
        queries = spread_heads(pairs_ref[b])
        scores = lax.dot_general(
            queries.astype(BF16), keys_ref[b], NT, preferred_element_type=F32
        )
        length = lengths_ref[b]
        sums = gates_ref[b]
        latest = jnp.sum(jnp.where(place == length - 1, sums, 0.0), axis=1, keepdims=True)
        fresh_gate = jnp.sum(jnp.where(column == b, gate_ref[...], 0.0), axis=1, keepdims=True)
        offsets = jnp.where(place < length, latest - sums + fresh_gate, -jnp.inf)
        wide = jnp.concatenate(
            [jnp.broadcast_to(offsets[:1], (16, slots)), jnp.broadcast_to(offsets[1:], (16, slots))], axis=0
        )
        scores = scores + wide
        fresh = fresh_ref[pl.ds(b, 1), :]
        own = jnp.sum(queries * fresh[:, : 2 * HEAD_LANES], axis=1, keepdims=True)
        state.append((scores, own, fresh[:, 2 * HEAD_LANES :]))
    for step, (scores, own, fresh_value) in enumerate(state):
        b = first + step
        highest = jnp.maximum(jnp.max(scores, axis=1, keepdims=True), own)
        past = jnp.exp(scores - highest)
        own = jnp.exp(own - highest)
        ratio = 1.0 / (jnp.sum(past, axis=1, keepdims=True) + own)
        weights = (past * ratio).astype(BF16)
        own_weight = (own * ratio).astype(BF16).astype(F32)
        mixed = jnp.dot(weights, values_ref[b], preferred_element_type=F32) + own_weight * fresh_value
        mixed_ref[b] = pair_heads(mixed)


class Transfers:
    def __init__(self):
        self.started = []

    def go(self, copy):
        copy.start()
        self.started.append(copy)

    def drain(self):
        for copy in self.started:
            copy.wait_send()


class Spread:
    def __init__(self, moves, view, core, spot, first, second, send1, recv1, send2, recv2):
        self.moves, self.view, self.core, self.spot = moves, view, core, spot
        self.first, self.second = first, second
        self.send1, self.recv1, self.send2, self.recv2 = send1, recv1, send2, recv2

    def near_copy(self, offset, source, target):
        region = self.view(source)
        return remote(region, region, self.send1.at[offset - 1], self.recv1.at[offset - 1], device_at(self.core, target))

    def far_copy(self, offset, piece, source, target):
        region = self.view(shifted(source, self.first, -piece))
        return remote(
            region, region, self.send2.at[offset - 1, piece], self.recv2.at[offset - 1, piece],
            device_at(self.core, target),
        )

    def far_start(self, piece):
        for offset in PIECES:
            self.moves.go(self.far_copy(offset, piece, self.spot, shifted(self.spot, self.second, offset)))

    def start(self):
        for offset in PIECES:
            self.moves.go(self.near_copy(offset, self.spot, shifted(self.spot, self.first, offset)))
        self.far_start(0)

    def relay(self, offset):
        self.near_copy(offset, shifted(self.spot, self.first, -offset), self.spot).wait_recv()
        self.far_start(offset)

    def far_arrive(self, offset):
        source = shifted(self.spot, self.second, -offset)
        for piece in range(SIDE):
            self.far_copy(offset, piece, source, self.spot).wait_recv()


def step_kernel(
    lengths_hbm, tokens_hbm, keys_hbm, values_hbm, gates_hbm, query_hbm, key_hbm, value_hbm, forget_hbm, ow_hbm,
    routes_hbm, shares_hbm, gate_hbm, up_hbm, down_hbm, dgate_hbm, dup_hbm, ddown_hbm,
    scale_hbm, gain_hbm, bias_hbm, out_ref,
    lengths_ref, tokens_ref, keys_ref, values_ref, gates_ref, wq_ref, wkv_ref, forget_ref, ow_ref, wo_ref,
    routes_ref, shares_ref, scale_ref, gain_ref, bias_ref,
    pairs_ref, mixed_ref, fresh_ref, newgate_ref, line_ref, sent_ref, back_ref, settled_ref,
    rows_ref, wg_ref, wu_ref, wd_ref, dense_ref, factor_ref, part_ref, r0_ref, r1_ref, r2_ref, s1_ref, s2_ref,
    asem, wsem, swsend, swrecv, xsend, xrecv, w1send, w1recv, w2send, w2recv,
    lsend, lrecv, bsend, brecv,
    g0send, g0recv, g1send, g1recv, g2send, g2recv,
    rsend, rrecv, r1send, r1recv, r2send, r2recv,
):
    core, spot = position()
    partner = device_at(1 - core, spot)
    entry_signal(core, spot)
    depth = WIDTH // GROUP
    first_loads = [(ow_hbm, ow_ref)]
    small = [
        (tokens_hbm, tokens_ref),
        (forget_hbm, forget_ref),
        (key_hbm, wkv_ref.at[:, pl.ds(0, 128)]),
        (value_hbm, wkv_ref.at[:, pl.ds(128, 128)]),
    ]
    wide = [(query_hbm.at[pl.ds(i * depth, depth)], wq_ref.at[pl.ds(i * depth, depth)]) for i in range(GROUP)]
    cache = [
        (keys_hbm, keys_ref), (values_hbm, values_ref), (gates_hbm, gates_ref), (lengths_hbm, lengths_ref),
        (gain_hbm, gain_ref), (bias_hbm, bias_ref), (scale_hbm, scale_ref),
        (routes_hbm, routes_ref), (shares_hbm, shares_ref),
    ]
    tables = ((gate_hbm, wg_ref), (up_hbm, wu_ref), (down_hbm, wd_ref))
    dense = (dgate_hbm, dup_hbm, ddown_hbm)
    shard = [(hbm, ref.at[core, pl.ds(0, FFE)]) for hbm, ref in tables]
    shard += [(hbm, dense_ref.at[core, i]) for i, hbm in enumerate(dense)]
    count = 0
    groups = []
    for group in (first_loads, small, wide, cache, shard):
        copies = []
        for source, target in group:
            copies.append(pltpu.make_async_copy(source, target, asem.at[count]))
            count += 1
        groups.append(copies)
    first_loads, small, wide, cache, shard = groups
    for load in first_loads + small + wide + cache:
        load.start()

    moves = Transfers()
    me = spot[2] * 2 + core

    def swap_copy(table, part, owner):
        hbm, ref = tables[table]
        size = FFE // 4
        here = pl.ds(part * size, size)
        return remote(
            hbm.at[here], ref.at[owner, here], swsend.at[table * 4 + part], swrecv.at[table * 4 + part], partner
        )

    def swap_dense(i, owner):
        return remote(dense[i], dense_ref.at[owner, i], swsend.at[12 + i], swrecv.at[12 + i], partner)

    def swap_start(table):
        for part in range(4):
            moves.go(swap_copy(table, part, core))
        moves.go(swap_dense(table, core))

    def line_target(offset, flip, sign=1):
        return (core if flip == 0 else 1 - core), shifted(spot, 2, sign * offset)

    def block_copy(index, from_core, source, to_core, target):
        z, y, x = source
        here = pl.multiple_of((target[2] * 2 + to_core) * PROJ, PROJ)
        return remote(
            ow_ref.at[:, pl.ds(here, PROJ)], wo_ref.at[z, y, x, from_core], xsend.at[index], xrecv.at[index],
            device_at(to_core, target),
        )

    for load in first_loads:
        load.wait()
    wo_ref[spot[0], spot[1], spot[2], core] = ow_ref[:, pl.ds(pl.multiple_of(me * PROJ, PROJ), PROJ)]
    entry_wait()
    for index, (offset, flip) in enumerate(LINE):
        moves.go(block_copy(index, core, spot, *line_target(offset, flip)))
    for load in shard:
        load.start()

    def weight_view(k):
        def view(source):
            return wo_ref.at[
                source[0], source[1], pl.ds(0, SIDE), pl.ds(0, 2), pl.ds(0, 2 * ROWS), pl.ds(k * HALF, HALF)
            ]

        return view

    weights = [
        Spread(
            moves, weight_view(k), core, spot, *WEIGHT_ORDER[k],
            w1send.at[k], w1recv.at[k], w2send.at[k], w2recv.at[k],
        )
        for k in range(2)
    ]

    for load in small:
        load.wait()
    tokens = tokens_ref[...]
    fresh_ref[...] = jnp.dot(tokens, wkv_ref[...], preferred_element_type=F32).astype(BF16).astype(F32)
    raw = lax.dot_general(forget_ref[...], tokens, NT, preferred_element_type=F32)
    newgate_ref[...] = jnp.minimum(raw, 0.0) - jnp.log1p(jnp.exp(-jnp.abs(raw)))
    query = jnp.zeros((ROWS, WIDTH), F32)
    for i in range(GROUP):
        wide[i].wait()
        query = query + jnp.dot(
            tokens[:, i * depth : (i + 1) * depth], wq_ref[i * depth : (i + 1) * depth, :], preferred_element_type=F32
        )
    query = query.astype(BF16).astype(F32) * HEAD_LANES**-0.5
    flat = pairs_ref.reshape(ROWS * 16, 128)
    for i in range(16):
        flat[pl.ds(i, ROWS, stride=16), :] = query[:, 128 * i : 128 * (i + 1)]
    for index, (offset, flip) in enumerate(LINE):
        from_core, source = line_target(offset, flip, -1)
        block_copy(index, from_core, source, core, spot).wait_recv()
    for weight in weights:
        weight.start()
    swap_start(0)
    for load in cache:
        load.wait()

    def some(i, carry):
        attend_some(
            i * ATTEND, ATTEND, lengths_ref, keys_ref, values_ref, gates_ref, pairs_ref, fresh_ref, newgate_ref,
            mixed_ref,
        )
        return carry

    lax.fori_loop(0, ROWS // ATTEND, some, 0)
    flat = mixed_ref.reshape(ROWS * 16, 128)
    attended = jnp.concatenate([flat[pl.ds(i, ROWS, stride=16), :] for i in range(16)], axis=1).astype(BF16)
    line_ref[spot[2], core] = attended

    def line_copy(index, from_core, source, to_core, target):
        here = line_ref.at[source[2], from_core]
        return remote(here, here, lsend.at[index], lrecv.at[index], device_at(to_core, target))

    for index, (offset, flip) in enumerate(LINE):
        moves.go(line_copy(index, core, spot, *line_target(offset, flip)))
    for offset in PIECES:
        for weight in weights:
            weight.relay(offset)
    swap_start(1)
    swap_start(2)

    expert = lax.axis_index("ep") // (2 * SIDE * SIDE * SIDE // EXPERTS)
    picked = jnp.where(routes_ref[...] == expert, shares_ref[...], 0.0)
    factor = jnp.sum(picked, axis=0, keepdims=True)
    turned = jnp.transpose(jnp.broadcast_to(factor, (8, factor.shape[1])))
    factor_ref[...] = turned.reshape(factor_ref.shape)

    for index, (offset, flip) in enumerate(LINE):
        from_core, source = line_target(offset, flip, -1)
        line_copy(index, from_core, source, core, spot).wait_recv()
    for offset in PIECES:
        for weight in weights:
            weight.far_arrive(offset)
    lines = line_ref.reshape(2 * SIDE * ROWS, WIDTH)[...]
    sent_ref.reshape(2 * SIDE * ROWS, PROJ)[...] = jnp.dot(
        lines, wo_ref.reshape(WIDTH, PROJ)[...], preferred_element_type=F32
    )

    def back_copy(index, from_core, source, to_core, target):
        return remote(
            sent_ref.at[target[2], to_core], back_ref.at[source[2], from_core], bsend.at[index], brecv.at[index],
            device_at(to_core, target),
        )

    for index, (offset, flip) in enumerate(LINE):
        moves.go(back_copy(index, core, spot, *line_target(offset, flip)))
    back_ref[spot[2], core] = sent_ref[spot[2], core]
    for index, (offset, flip) in enumerate(LINE):
        from_core, source = line_target(offset, flip, -1)
        back_copy(index, from_core, source, core, spot).wait_recv()
    projected = jnp.concatenate([back_ref[i // 2, i % 2] for i in range(2 * SIDE)], axis=1)
    settled = norm_rows(residual_scale * tokens.astype(F32) + projected, gain_ref[0:1, :], bias_ref[0:1, :])
    settled_ref[...] = settled
    rows_ref[spot] = settled

    def row_view(k):
        gone = GATHER_ORDER[k][0]

        def view(source):
            where = tuple(pl.ds(0, SIDE) if d == gone else source[d] for d in range(3))
            return rows_ref.at[where + (pl.ds(0, ROWS), columns(k))]

        return view

    def first_copy(k, offset, source, target):
        region = rows_ref.at[source + (pl.ds(0, ROWS), columns(k))]
        return remote(region, region, g0send.at[k, offset - 1], g0recv.at[k, offset - 1], device_at(core, target))

    for offset in PIECES:
        for k in range(3):
            moves.go(first_copy(k, offset, spot, shifted(spot, GATHER_ORDER[k][0], offset)))

    pad = jnp.zeros((FFP - FFE - FFD, WIDTH), BF16)

    def dense_rows(slot):
        for i, ref in ((0, wg_ref), (1, wu_ref), (2, wd_ref)):
            value = dense_ref[slot, i]
            if i == 2:
                value = (value.astype(F32) * scale_ref[...]).astype(BF16)
            ref[slot, FFE:, :] = jnp.concatenate([value, pad], axis=0)

    for load in shard:
        load.wait()
    dense_rows(core)
    spreads = [
        Spread(
            moves, row_view(k), core, spot, *GATHER_ORDER[k][1:],
            g1send.at[k], g1recv.at[k], g2send.at[k], g2recv.at[k],
        )
        for k in range(3)
    ]
    for k in range(3):
        for offset in PIECES:
            first_copy(k, offset, shifted(spot, GATHER_ORDER[k][0], -offset), spot).wait_recv()
        spreads[k].start()
    for offset in PIECES:
        for k in range(3):
            spreads[k].relay(offset)
    for table in range(3):
        for part in range(4):
            swap_copy(table, part, 1 - core).wait_recv()
        swap_dense(table, 1 - core).wait_recv()
    dense_rows(1 - core)
    for offset in PIECES:
        for k in range(3):
            spreads[k].far_arrive(offset)

    block = 2 * SIDE * SIDE * ROWS
    lane = lax.broadcasted_iota(jnp.int32, (1, 2 * FFP), 1) % FFP

    def ffn(i, carry):
        x = rows_ref.at[pl.ds(2 * i, 2)].reshape(block, WIDTH)[...]
        gate = lax.dot_general(x, wg_ref.reshape(2 * FFP, WIDTH)[...], NT, preferred_element_type=F32)
        up = lax.dot_general(x, wu_ref.reshape(2 * FFP, WIDTH)[...], NT, preferred_element_type=F32)
        weight = factor_ref[pl.ds(2 * i * SIDE * SIDE, 2 * SIDE * SIDE), core].reshape(block, 8)[:, :1]
        weight = jnp.where(lane < FFE, weight, 1.0)
        hidden = (gate * jax.nn.sigmoid(gate) * up * weight).astype(BF16)
        value = jnp.dot(hidden, wd_ref.reshape(2 * FFP, WIDTH)[...], preferred_element_type=F32)
        part_ref.at[pl.ds(2 * i, 2)].reshape(block, WIDTH)[...] = value.astype(BF16)
        return carry

    lax.fori_loop(0, SIDE // 2, ffn, 0)

    def dims_of(k):
        return GATHER_ORDER[k][::-1]

    def cell(ref, lead, k, phase, fixed):
        gone = dims_of(k)[:phase]
        where = tuple(fixed.get(d, pl.ds(0, SIDE)) for d in range(3) if d not in gone)
        return ref.at[lead + where + (pl.ds(0, ROWS), columns(k))]

    def send0(k, offset, piece, target):
        a, b, _ = dims_of(k)
        line = (spot[b] + piece) % SIDE
        return remote(
            cell(part_ref, (), k, 0, {a: target[a], b: line}), cell(r0_ref, (offset - 1,), k, 1, {b: line}),
            rsend.at[k, offset - 1, piece], rrecv.at[k, offset - 1, piece], device_at(core, target),
        )

    def send1(k, offset, target):
        b = dims_of(k)[1]
        return remote(
            cell(s1_ref, (), k, 1, {b: target[b]}), cell(r1_ref, (offset - 1,), k, 2, {}),
            r1send.at[k, offset - 1], r1recv.at[k, offset - 1], device_at(core, target),
        )

    def send2(k, offset, target):
        c = dims_of(k)[2]
        return remote(
            cell(s2_ref, (), k, 2, {c: target[c]}), cell(r2_ref, (offset - 1,), k, 3, {}),
            r2send.at[k, offset - 1], r2recv.at[k, offset - 1], device_at(core, target),
        )

    order = (2, 1, 3, 0)
    for piece in order:
        for offset in PIECES:
            for k in range(3):
                moves.go(send0(k, offset, piece, shifted(spot, dims_of(k)[0], offset)))
    for piece in order:
        for k in range(3):
            a, b, _ = dims_of(k)
            line = (spot[b] + piece) % SIDE
            total = cell(part_ref, (), k, 0, {a: spot[a], b: line})[...].astype(F32)
            for offset in PIECES:
                send0(k, offset, piece, spot).wait_recv()
                total = total + cell(r0_ref, (offset - 1,), k, 1, {b: line})[...].astype(F32)
            cell(s1_ref, (), k, 1, {b: line})[...] = total.astype(BF16)
            if piece:
                moves.go(send1(k, piece, shifted(spot, b, piece)))
    for k in range(3):
        b, c = dims_of(k)[1:]
        total = cell(s1_ref, (), k, 1, {b: spot[b]})[...].astype(F32)
        for offset in PIECES:
            send1(k, offset, spot).wait_recv()
            total = total + cell(r1_ref, (offset - 1,), k, 2, {})[...].astype(F32)
        cell(s2_ref, (), k, 2, {})[...] = total.astype(BF16)
        for offset in PIECES:
            moves.go(send2(k, offset, shifted(spot, c, offset)))
    sums = []
    for k in range(3):
        c = dims_of(k)[2]
        total = cell(s2_ref, (), k, 2, {c: spot[c]})[...].astype(F32)
        for offset in PIECES:
            send2(k, offset, spot).wait_recv()
            total = total + cell(r2_ref, (offset - 1,), k, 3, {})[...].astype(F32)
        sums.append(total)
    ffn_sum = jnp.concatenate(sums, axis=-1)
    out_ref[...] = norm_rows(
        residual_scale * settled_ref[...].astype(F32) + ffn_sum, gain_ref[1:2, :], bias_ref[1:2, :]
    )
    moves.drain()


def step_call(*operands):
    vmem = pl.BlockSpec(memory_space=pltpu.VMEM)
    hbm = pl.BlockSpec(memory_space=pltpu.HBM)
    sem = pltpu.SemaphoreType.DMA
    cube = (SIDE, SIDE, SIDE, ROWS, WIDTH)
    slots = operands[2].shape[1]
    line = len(LINE)
    return pl.pallas_call(
        step_kernel,
        out_shape=jax.ShapeDtypeStruct((ROWS, WIDTH), BF16),
        in_specs=[hbm] * len(operands),
        out_specs=vmem,
        scratch_shapes=[
            pltpu.SMEM((ROWS,), jnp.int32),
            pltpu.VMEM((ROWS, WIDTH), BF16),
            pltpu.VMEM((ROWS, slots, 128), BF16),
            pltpu.VMEM((ROWS, slots, 128), BF16),
            pltpu.VMEM((ROWS, 2, slots), F32),
            pltpu.VMEM((WIDTH, WIDTH), BF16),
            pltpu.VMEM((WIDTH, 256), BF16),
            pltpu.VMEM((2, WIDTH), BF16),
            pltpu.VMEM((2 * ROWS, WIDTH), BF16),
            pltpu.VMEM((SIDE, SIDE, SIDE, 2, 2 * ROWS, PROJ), BF16),
            pltpu.VMEM((2, 2 * SIDE**3 * ROWS), jnp.int32),
            pltpu.VMEM((2, 2 * SIDE**3 * ROWS), F32),
            pltpu.VMEM((1, WIDTH), F32),
            pltpu.VMEM((2, WIDTH), F32),
            pltpu.VMEM((2, WIDTH), F32),
            pltpu.VMEM((ROWS, 16, 128), F32),
            pltpu.VMEM((ROWS, 16, 128), F32),
            pltpu.VMEM((ROWS, 256), F32),
            pltpu.VMEM((2, ROWS), F32),
            pltpu.VMEM((SIDE, 2, ROWS, WIDTH), BF16),
            pltpu.VMEM((SIDE, 2, ROWS, PROJ), F32),
            pltpu.VMEM((SIDE, 2, ROWS, PROJ), F32),
            pltpu.VMEM((ROWS, WIDTH), BF16),
            pltpu.VMEM(cube, BF16),
            pltpu.VMEM((2, FFP, WIDTH), BF16),
            pltpu.VMEM((2, FFP, WIDTH), BF16),
            pltpu.VMEM((2, FFP, WIDTH), BF16),
            pltpu.VMEM((2, 3, FFD, WIDTH), BF16),
            pltpu.VMEM((SIDE**3, 2, ROWS, 8), F32),
            pltpu.VMEM(cube, BF16),
            pltpu.VMEM((PEERS,) + cube[1:], BF16),
            pltpu.VMEM((PEERS,) + cube[2:], BF16),
            pltpu.VMEM((PEERS,) + cube[3:], BF16),
            pltpu.VMEM(cube[1:], BF16),
            pltpu.VMEM(cube[2:], BF16),
            sem((24,)), sem((1,)), sem((15,)), sem((15,)),
            sem((line,)), sem((line,)),
            sem((2, PEERS)), sem((2, PEERS)), sem((2, PEERS, SIDE)), sem((2, PEERS, SIDE)),
            sem((line,)), sem((line,)), sem((line,)), sem((line,)),
            sem((3, PEERS)), sem((3, PEERS)),
            sem((3, PEERS)), sem((3, PEERS)), sem((3, PEERS, SIDE)), sem((3, PEERS, SIDE)),
            sem((3, PEERS, SIDE)), sem((3, PEERS, SIDE)),
            sem((3, PEERS)), sem((3, PEERS)), sem((3, PEERS)), sem((3, PEERS)),
        ],
        compiler_params=pltpu.CompilerParams(
            collective_id=0, has_side_effects=True, vmem_limit_bytes=60 * 2**20
        ),
        name="step",
    )(*operands)


def local(
    tokens,
    cache_keys,
    cache_values,
    cum_gates,
    lengths,
    query_weight,
    key_weight,
    value_weight,
    forget_weight,
    out_weight,
    norm_gain,
    norm_bias,
    dense_gate_weight,
    dense_up_weight,
    dense_down_weight,
    dense_scale,
    expert_gate_weight,
    expert_up_weight,
    expert_down_weight,
    routes,
    route_weights,
):
    return step_call(
        lengths,
        tokens,
        cache_keys,
        cache_values,
        jnp.transpose(cum_gates, (0, 2, 1)),
        query_weight,
        key_weight,
        value_weight,
        jnp.transpose(forget_weight),
        out_weight,
        jnp.transpose(routes),
        jnp.transpose(route_weights),
        jnp.transpose(expert_gate_weight),
        jnp.transpose(expert_up_weight),
        expert_down_weight,
        jnp.transpose(dense_gate_weight),
        jnp.transpose(dense_up_weight),
        dense_down_weight,
        dense_scale.reshape(1, -1),
        norm_gain,
        norm_bias,
    )


def solution(mesh):
    return jax.shard_map(
        local,
        mesh=mesh,
        in_specs=(
            P("ep", None),
            P("ep", None, None),
            P("ep", None, None),
            P("ep", None, None),
            P("ep"),
            P(),
            P(),
            P(),
            P(),
            P("ep", None),
            P(),
            P(),
            P(None, "ep"),
            P(None, "ep"),
            P("ep", None),
            P(),
            P(None, "ep"),
            P(None, "ep"),
            P("ep", None),
            P(),
            P(),
        ),
        out_specs=P("ep", None),
        check_vma=False,
    )
```

time: 82.8 us -> 71.3 us (0.86)
  Pallas kernels: 81.3 us -> 69.8 us
    pallas_call x1, Pallas kernels: 81.3 us -> 69.8 us  [step_call(): pl.pallas_call(step_kernel, out_shape=jax.ShapeDtypeStruct((ROWS, WIDTH),...]
where the time goes in v3:
time: 71.3 us; the launch traced here: 71.2 us
  Pallas kernels  69.8 us (98%)
  local copies, waits for them, and re-layouts  1.38 us (2%)
    pallas_call x1, Pallas kernels, step_call(): pl.pallas_call(step_kernel, out_shape=jax.ShapeDtypeStruct((ROWS, WIDTH),...  69.8 us

profile of v3, /device:TPU:0, one launch (start us, length us, event | category | flops | bytes accessed | tf_op | source)
XLA Modules:
  0.0 71.2 jit_solution(13793192100123777683)
XLA Ops:
  0.0 69.8 %step.1 = bf16[8,2048]{1,0:T(8,128)(2,1)} custom-call(s32[8]{0:T(128)} %lengths_hbm.1, bf16[8,2048]{1,0:T(8,128)(2,1)} %tokens_hbm.1, bf16[8,1024,128]{2,1,0:T(8,128)(2,1)} %keys_hbm.1, bf16[8,1024,128]{2,1,0:T(8,128)(2,1)} %values_hbm.1, f32[8,2,1024]{2,1,0:T(2,128)} %bitcast.13, bf16[2048,2048]{1,0:T(8,128)(2,1)} %query_hbm.1, bf16[2048,128]{1,0:T(8,128)(2,1)} %key_hbm.1, ...), custom_call_target="tpu_custom_call" | custom-call | tf_op jit(solution)/shard_map/step/pallas_call | solution.py:530
  69.8 1.4 %copy.23 = bf16[8,2048]{1,0:T(8,128)(2,1)} copy(bf16[8,2048]{1,0:T(8,128)(2,1)} %step.1) | data formatting | bytes 65536

commit v4 on v3

--- a/solution.py
+++ b/solution.py
@@ -18,6 +18,7 @@
 FFD = 44
 FFP = 512
 CHUNKS = ((0, 768), (768, 640), (1408, 640))
+REDUCE_CHUNKS = ((0, 768), (768, 512), (1280, 768))
 GATHER_ORDER = ((2, 1, 0), (0, 2, 1), (1, 0, 2))
 ATTEND = 4
 residual_scale = 1.4142135
@@ -205,7 +206,7 @@
     lengths_ref, tokens_ref, keys_ref, values_ref, gates_ref, wq_ref, wkv_ref, forget_ref, ow_ref, wo_ref,
     routes_ref, shares_ref, scale_ref, gain_ref, bias_ref,
     pairs_ref, mixed_ref, fresh_ref, newgate_ref, line_ref, sent_ref, back_ref, settled_ref,
-    rows_ref, wg_ref, wu_ref, wd_ref, dense_ref, factor_ref, part_ref, r0_ref, r1_ref, r2_ref, s1_ref, s2_ref,
+    rows_ref, wg_ref, wu_ref, wd_ref, dense_ref, factor_ref, hidden_ref, part_ref, r0_ref, r1_ref, r2_ref, s1_ref, s2_ref,
     asem, wsem, swsend, swrecv, xsend, xrecv, w1send, w1recv, w2send, w2recv,
     lsend, lrecv, bsend, brecv,
     g0send, g0recv, g1send, g1recv, g2send, g2recv,
@@ -434,21 +435,34 @@
         for k in range(3):
             spreads[k].far_arrive(offset)
 
-    block = 2 * SIDE * SIDE * ROWS
+    plane_rows = SIDE * SIDE * ROWS
+    block = 2 * plane_rows
     lane = lax.broadcasted_iota(jnp.int32, (1, 2 * FFP), 1) % FFP
-
-    def ffn(i, carry):
-        x = rows_ref.at[pl.ds(2 * i, 2)].reshape(block, WIDTH)[...]
-        gate = lax.dot_general(x, wg_ref.reshape(2 * FFP, WIDTH)[...], NT, preferred_element_type=F32)
-        up = lax.dot_general(x, wu_ref.reshape(2 * FFP, WIDTH)[...], NT, preferred_element_type=F32)
-        weight = factor_ref[pl.ds(2 * i * SIDE * SIDE, 2 * SIDE * SIDE), core].reshape(block, 8)[:, :1]
+    wg_all, wu_all, wd_all = (ref.reshape(2 * FFP, WIDTH) for ref in (wg_ref, wu_ref, wd_ref))
+
+    def plane(offset):
+        return shifted(spot, 0, offset)[0]
+
+    def hidden_block(i, carry):
+        pair = (plane(2 + i), plane(1 - i))
+        x = jnp.concatenate([rows_ref.at[p].reshape(plane_rows, WIDTH)[...] for p in pair], axis=0)
+        gate = lax.dot_general(x, wg_all[...], NT, preferred_element_type=F32)
+        up = lax.dot_general(x, wu_all[...], NT, preferred_element_type=F32)
+        weight = jnp.concatenate(
+            [factor_ref[pl.ds(p * SIDE * SIDE, SIDE * SIDE), core].reshape(plane_rows, 8)[:, :1] for p in pair], axis=0
+        )
         weight = jnp.where(lane < FFE, weight, 1.0)
-        hidden = (gate * jax.nn.sigmoid(gate) * up * weight).astype(BF16)
-        value = jnp.dot(hidden, wd_ref.reshape(2 * FFP, WIDTH)[...], preferred_element_type=F32)
-        part_ref.at[pl.ds(2 * i, 2)].reshape(block, WIDTH)[...] = value.astype(BF16)
+        hidden_ref[...] = (gate * jax.nn.sigmoid(gate) * up * weight).astype(BF16)
         return carry
 
-    lax.fori_loop(0, SIDE // 2, ffn, 0)
+    def down(i, k):
+        here = span(k)
+        value = jnp.dot(hidden_ref[...], wd_all[:, here], preferred_element_type=F32).astype(BF16)
+        for n, p in enumerate((plane(2 + i), plane(1 - i))):
+            part_ref.at[p].reshape(plane_rows, WIDTH)[:, here] = value[n * plane_rows : (n + 1) * plane_rows]
+
+    def span(k):
+        return pl.ds(REDUCE_CHUNKS[k][0], REDUCE_CHUNKS[k][1])
 
     def dims_of(k):
         return GATHER_ORDER[k][::-1]
@@ -456,7 +470,7 @@
     def cell(ref, lead, k, phase, fixed):
         gone = dims_of(k)[:phase]
         where = tuple(fixed.get(d, pl.ds(0, SIDE)) for d in range(3) if d not in gone)
-        return ref.at[lead + where + (pl.ds(0, ROWS), columns(k))]
+        return ref.at[lead + where + (pl.ds(0, ROWS), span(k))]
 
     def send0(k, offset, piece, target):
         a, b, _ = dims_of(k)
@@ -480,22 +494,38 @@
             r2send.at[k, offset - 1], r2recv.at[k, offset - 1], device_at(core, target),
         )
 
+    def send_part(k, offsets, pieces):
+        for piece in pieces:
+            for offset in offsets:
+                moves.go(send0(k, offset, piece, shifted(spot, dims_of(k)[0], offset)))
+
+    def sum_part(k, piece):
+        a, b, _ = dims_of(k)
+        line = (spot[b] + piece) % SIDE
+        total = cell(part_ref, (), k, 0, {a: spot[a], b: line})[...].astype(F32)
+        for offset in PIECES:
+            send0(k, offset, piece, spot).wait_recv()
+            total = total + cell(r0_ref, (offset - 1,), k, 1, {b: line})[...].astype(F32)
+        cell(s1_ref, (), k, 1, {b: line})[...] = total.astype(BF16)
+        if piece:
+            moves.go(send1(k, piece, shifted(spot, b, piece)))
+
     order = (2, 1, 3, 0)
-    for piece in order:
-        for offset in PIECES:
-            for k in range(3):
-                moves.go(send0(k, offset, piece, shifted(spot, dims_of(k)[0], offset)))
-    for piece in order:
-        for k in range(3):
-            a, b, _ = dims_of(k)
-            line = (spot[b] + piece) % SIDE
-            total = cell(part_ref, (), k, 0, {a: spot[a], b: line})[...].astype(F32)
-            for offset in PIECES:
-                send0(k, offset, piece, spot).wait_recv()
-                total = total + cell(r0_ref, (offset - 1,), k, 1, {b: line})[...].astype(F32)
-            cell(s1_ref, (), k, 1, {b: line})[...] = total.astype(BF16)
-            if piece:
-                moves.go(send1(k, piece, shifted(spot, b, piece)))
+    hidden_block(0, 0)
+    down(0, 0)
+    send_part(0, (1, 2), order)
+    down(0, 2)
+    send_part(2, PIECES, (2, 1))
+    down(0, 1)
+    hidden_block(1, 0)
+    down(1, 1)
+    send_part(1, PIECES, order)
+    down(1, 0)
+    send_part(0, (3,), order)
+    down(1, 2)
+    send_part(2, PIECES, (3, 0))
+    for k, piece in ((2, 2), (2, 1), (1, 2), (0, 2), (1, 1), (0, 1), (2, 3), (1, 3), (0, 3), (2, 0), (1, 0), (0, 0)):
+        sum_part(k, piece)
     for k in range(3):
         b, c = dims_of(k)[1:]
         total = cell(s1_ref, (), k, 1, {b: spot[b]})[...].astype(F32)
@@ -562,6 +592,7 @@
             pltpu.VMEM((2, FFP, WIDTH), BF16),
             pltpu.VMEM((2, 3, FFD, WIDTH), BF16),
             pltpu.VMEM((SIDE**3, 2, ROWS, 8), F32),
+            pltpu.VMEM((2 * SIDE * SIDE * ROWS, 2 * FFP), BF16),
             pltpu.VMEM(cube, BF16),
             pltpu.VMEM((PEERS,) + cube[1:], BF16),
             pltpu.VMEM((PEERS,) + cube[2:], BF16),

time: 71.3 us -> 68.2 us (0.957)
  Pallas kernels: 69.8 us -> 66.7 us
    pallas_call x1, Pallas kernels: 69.8 us -> 66.7 us  [step_call(): pl.pallas_call(step_kernel, out_shape=jax.ShapeDtypeStruct((ROWS, WIDTH),...]
where the time goes in v4:
time: 68.2 us; the launch traced here: 68.1 us
  Pallas kernels  66.7 us (98%)
  local copies, waits for them, and re-layouts  1.38 us (2%)
    pallas_call x1, Pallas kernels, step_call(): pl.pallas_call(step_kernel, out_shape=jax.ShapeDtypeStruct((ROWS, WIDTH),...  66.7 us
    unnamed x1, local copies, waits for them, and re-layouts  1.38 us

profile of v4, /device:TPU:0, one launch (start us, length us, event | category | flops | bytes accessed | tf_op | source)
XLA Modules:
  0.0 68.1 jit_solution(8099675467725145458)
XLA Ops:
  0.0 66.7 %step.1 = bf16[8,2048]{1,0:T(8,128)(2,1)} custom-call(s32[8]{0:T(128)} %lengths_hbm.1, bf16[8,2048]{1,0:T(8,128)(2,1)} %tokens_hbm.1, bf16[8,1024,128]{2,1,0:T(8,128)(2,1)} %keys_hbm.1, bf16[8,1024,128]{2,1,0:T(8,128)(2,1)} %values_hbm.1, f32[8,2,1024]{2,1,0:T(2,128)} %bitcast.13, bf16[2048,2048]{1,0:T(8,128)(2,1)} %query_hbm.1, bf16[2048,128]{1,0:T(8,128)(2,1)} %key_hbm.1, ...), custom_call_target="tpu_custom_call" | custom-call | tf_op jit(solution)/shard_map/step/pallas_call | solution.py:560
  66.7 1.4 %copy.23 = bf16[8,2048]{1,0:T(8,128)(2,1)} copy(bf16[8,2048]{1,0:T(8,128)(2,1)} %step.1) | data formatting | bytes 65536

commit v5 on v4

--- a/solution.py
+++ b/solution.py
@@ -89,7 +89,8 @@
 HEAD_LANES = 64
 PEERS = SIDE - 1
 PIECES = (1, 3, 2)
-LINE = tuple((offset, flip) for offset in range(SIDE) for flip in range(2))[1:]
+FAR_FIRST = (2, 1, 3)
+LINE = tuple((offset, flip) for offset in FAR_FIRST + (0,) for flip in range(2) if offset or flip)
 
 
 def spread_heads(pairs):
@@ -161,6 +162,7 @@
     def drain(self):
         for copy in self.started:
             copy.wait_send()
+        self.started = []
 
 
 class Spread:
@@ -181,7 +183,7 @@
         )
 
     def far_start(self, piece):
-        for offset in PIECES:
+        for offset in FAR_FIRST:
             self.moves.go(self.far_copy(offset, piece, self.spot, shifted(self.spot, self.second, offset)))
 
     def start(self):
@@ -396,7 +398,7 @@
         region = rows_ref.at[source + (pl.ds(0, ROWS), columns(k))]
         return remote(region, region, g0send.at[k, offset - 1], g0recv.at[k, offset - 1], device_at(core, target))
 
-    for offset in PIECES:
+    for offset in FAR_FIRST:
         for k in range(3):
             moves.go(first_copy(k, offset, spot, shifted(spot, GATHER_ORDER[k][0], offset)))
 
@@ -511,20 +513,25 @@
             moves.go(send1(k, piece, shifted(spot, b, piece)))
 
     order = (2, 1, 3, 0)
+    before = len(moves.started)
     hidden_block(0, 0)
     down(0, 0)
-    send_part(0, (1, 2), order)
+    send_part(0, (2, 1), order)
     down(0, 2)
-    send_part(2, PIECES, (2, 1))
+    send_part(2, FAR_FIRST, (2, 1))
     down(0, 1)
     hidden_block(1, 0)
     down(1, 1)
-    send_part(1, PIECES, order)
+    send_part(1, FAR_FIRST, order)
     down(1, 0)
     send_part(0, (3,), order)
     down(1, 2)
-    send_part(2, PIECES, (3, 0))
-    for k, piece in ((2, 2), (2, 1), (1, 2), (0, 2), (1, 1), (0, 1), (2, 3), (1, 3), (0, 3), (2, 0), (1, 0), (0, 0)):
+    early = moves.started[:before]
+    moves.started = moves.started[before:]
+    send_part(2, FAR_FIRST, (3, 0))
+    for copy in early:
+        copy.wait_send()
+    for k, piece in ((2, 2), (2, 1), (1, 2), (1, 1), (0, 2), (0, 1), (1, 3), (0, 3), (2, 3), (1, 0), (0, 0), (2, 0)):
         sum_part(k, piece)
     for k in range(3):
         b, c = dims_of(k)[1:]
@@ -533,8 +540,9 @@
             send1(k, offset, spot).wait_recv()
             total = total + cell(r1_ref, (offset - 1,), k, 2, {})[...].astype(F32)
         cell(s2_ref, (), k, 2, {})[...] = total.astype(BF16)
-        for offset in PIECES:
+        for offset in FAR_FIRST:
             moves.go(send2(k, offset, shifted(spot, c, offset)))
+    moves.drain()
     sums = []
     for k in range(3):
         c = dims_of(k)[2]

time: 68.2 us -> 66.6 us (0.977)
  Pallas kernels: 66.7 us -> 65 us
    pallas_call x1, Pallas kernels: 66.7 us -> 65 us  [step_call(): pl.pallas_call(step_kernel, out_shape=jax.ShapeDtypeStruct((ROWS, WIDTH),...]
where the time goes in v5:
time: 66.6 us; the launch traced here: 66.4 us
  Pallas kernels  65 us (98%)
  local copies, waits for them, and re-layouts  1.38 us (2%)
    pallas_call x1, Pallas kernels, step_call(): pl.pallas_call(step_kernel, out_shape=jax.ShapeDtypeStruct((ROWS, WIDTH),...  65 us
    unnamed x1, local copies, waits for them, and re-layouts  1.38 us

profile of v5, /device:TPU:0, one launch (start us, length us, event | category | flops | bytes accessed | tf_op | source)
XLA Modules:
  0.0 66.4 jit_solution(10945707782270844616)
XLA Ops:
  0.0 65.0 %step.1 = bf16[8,2048]{1,0:T(8,128)(2,1)} custom-call(s32[8]{0:T(128)} %lengths_hbm.1, bf16[8,2048]{1,0:T(8,128)(2,1)} %tokens_hbm.1, bf16[8,1024,128]{2,1,0:T(8,128)(2,1)} %keys_hbm.1, bf16[8,1024,128]{2,1,0:T(8,128)(2,1)} %values_hbm.1, f32[8,2,1024]{2,1,0:T(2,128)} %bitcast.13, bf16[2048,2048]{1,0:T(8,128)(2,1)} %query_hbm.1, bf16[2048,128]{1,0:T(8,128)(2,1)} %key_hbm.1, ...), custom_call_target="tpu_custom_call" | custom-call | tf_op jit(solution)/shard_map/step/pallas_call | solution.py:568
  65.1 1.4 %copy.23 = bf16[8,2048]{1,0:T(8,128)(2,1)} copy(bf16[8,2048]{1,0:T(8,128)(2,1)} %step.1) | data formatting | bytes 65536

commit v6 on v5

--- a/solution.py
+++ b/solution.py
@@ -552,10 +552,13 @@
             total = total + cell(r2_ref, (offset - 1,), k, 3, {})[...].astype(F32)
         sums.append(total)
     ffn_sum = jnp.concatenate(sums, axis=-1)
-    out_ref[...] = norm_rows(
+    settled_ref[...] = norm_rows(
         residual_scale * settled_ref[...].astype(F32) + ffn_sum, gain_ref[1:2, :], bias_ref[1:2, :]
     )
+    last = pltpu.make_async_copy(settled_ref, out_ref, wsem.at[0])
+    last.start()
     moves.drain()
+    last.wait()
 
 
 def step_call(*operands):
@@ -569,7 +572,7 @@
         step_kernel,
         out_shape=jax.ShapeDtypeStruct((ROWS, WIDTH), BF16),
         in_specs=[hbm] * len(operands),
-        out_specs=vmem,
+        out_specs=hbm,
         scratch_shapes=[
             pltpu.SMEM((ROWS,), jnp.int32),
             pltpu.VMEM((ROWS, WIDTH), BF16),

time: 66.6 us -> 66.6 us (level)
  no operation moved by 1% of the time
where the time goes in v6:
time: 66.6 us; the launch traced here: 66.4 us
  Pallas kernels  65 us (98%)
  local copies, waits for them, and re-layouts  1.38 us (2%)
    pallas_call x1, Pallas kernels, step_call(): pl.pallas_call(step_kernel, out_shape=jax.ShapeDtypeStruct((ROWS, WIDTH),...  65 us
    unnamed x1, local copies, waits for them, and re-layouts  1.38 us

profile of v6, /device:TPU:0, one launch (start us, length us, event | category | flops | bytes accessed | tf_op | source)
XLA Modules:
  0.0 66.4 jit_solution(14206150279838457912)
XLA Ops:
  0.0 65.0 %step.1 = bf16[8,2048]{1,0:T(8,128)(2,1)} custom-call(s32[8]{0:T(128)} %lengths_hbm.1, bf16[8,2048]{1,0:T(8,128)(2,1)} %tokens_hbm.1, bf16[8,1024,128]{2,1,0:T(8,128)(2,1)} %keys_hbm.1, bf16[8,1024,128]{2,1,0:T(8,128)(2,1)} %values_hbm.1, f32[8,2,1024]{2,1,0:T(2,128)} %bitcast.13, bf16[2048,2048]{1,0:T(8,128)(2,1)} %query_hbm.1, bf16[2048,128]{1,0:T(8,128)(2,1)} %key_hbm.1, ...), custom_call_target="tpu_custom_call" | custom-call | tf_op jit(solution)/shard_map/step/pallas_call | solution.py:571
  65.0 1.4 %copy.23 = bf16[8,2048]{1,0:T(8,128)(2,1)} copy(bf16[8,2048]{1,0:T(8,128)(2,1)} %step.1) | data formatting | bytes 65536
